TPU v7x, 256 devices: a whole 4x4x8 slice. The times are simulated.
256 devices in a mesh: sp: 16 (over y, x), tp: 16 (over z, core).
Axes of the slice: x: 4, y: 4, z: 8, core: 2. Of those that a mesh axis runs over, the one named last changes fastest.
Arguments:
- conv_value: bfloat16 [1024, 16384], P('tp', 'sp'), may hold values from -6 to 6
- conv_gate: bfloat16 [1024, 16384], P('tp', 'sp'), may hold values from -6 to 6
- conv_taps: float32 [1024, 31], P('tp'), may hold values from -2.2 to 2.2
- norm_gain: float32 [1024], replicated, may hold values from 0.1 to 1.9
- norm_bias: float32 [1024], replicated, may hold values from -3 to 3
- out_weight: bfloat16 [1024, 2048], replicated, may hold values from -0.1875 to 0.1875
- stream: bfloat16 [16384, 2048], P(('sp', 'tp')), may hold values from -6 to 6
- routes: int32 [16384, 2], P(('sp', 'tp')), may hold values from 0 to 15, all different within a row; in each aligned block of 64 rows (0 to 63, 64 to 127, ...) at most 8 rows name the same one
- route_weights: float32 [16384, 2], P(('sp', 'tp')), may hold values from 0.2 to 1
- expert_gain: float32 [2048], replicated, may hold values from 0.1 to 1.9
- expert_gate: bfloat16 [16, 2048, 7168], P('sp', None, 'tp'), may hold values from -0.125 to 0.125
- expert_up: bfloat16 [16, 2048, 7168], P('sp', None, 'tp'), may hold values from -0.125 to 0.125
- expert_down: bfloat16 [16, 7168, 2048], P('sp', 'tp'), may hold values from -0.0625 to 0.0625
Outputs:
- mixed: bfloat16 [16384, 2048], P(('sp', 'tp'))
Inputs may be any that keep to these rules, and one draw needn't show every extreme that they name: `routes`: within each device's 64 rows every expert is named exactly 8 times; a row names distinct experts.
All inputs are finite; a program needn't handle non-finite values.
Results may differ from a plain program's by a relative error of at most 0.014.
Values may be sent and summed in bfloat16 or wider, within the bound.
A program may use at most 64 MiB of HBM per device.

v0:
```python
import jax
import jax.numpy as jnp
from jax import lax
from jax.sharding import PartitionSpec as P

epsilon = 1e-06


def shifted(value, axis, steps):
    count = lax.axis_size(axis)
    initial, last = (max(0, -steps), min(count, count - steps))
    return lax.ppermute(value, axis, [(source, source + steps) for source in range(initial, last)])


def per_device(
    conv_value,
    conv_gate,
    conv_taps,
    norm_gain,
    norm_bias,
    out_weight,
    stream,
    routes,
    route_weights,
    expert_gain,
    expert_gate,
    expert_up,
    expert_down,
):
    f32 = jnp.float32
    local_ch = conv_value.shape[0]
    run_len = conv_value.shape[1]
    kernel_len = conv_taps.shape[1]
    gated_input = (conv_value.astype(f32) * jax.nn.sigmoid(conv_gate.astype(f32))).astype(
        jnp.bfloat16
    )
    left_rim = shifted(gated_input[:, run_len - (kernel_len - 1) :], "sp", 1)
    padded = jnp.concatenate([left_rim, gated_input], axis=1).astype(f32)
    conv_sum = jnp.zeros((local_ch, run_len), f32)
    for offset in range(kernel_len):
        conv_sum = (
            conv_sum + conv_taps[:, offset : offset + 1] * padded[:, offset : offset + run_len]
        )
    conv_out = conv_sum.astype(jnp.bfloat16)
    whole_conv = lax.all_to_all(conv_out, "tp", split_axis=1, concat_axis=0, tiled=True).astype(f32)
    center = jnp.mean(whole_conv, axis=0, keepdims=True)
    spread = jnp.mean((whole_conv - center) ** 2, axis=0, keepdims=True)
    scaled = (whole_conv - center) * lax.rsqrt(spread + epsilon) * norm_gain[:, None] + norm_bias[
        :, None
    ]
    token_major = jax.nn.silu(scaled).astype(jnp.bfloat16)
    projected = lax.dot_general(
        token_major, out_weight, (((0,), (0,)), ((), ())), preferred_element_type=f32
    )
    residual = (stream.astype(f32) + projected).astype(jnp.bfloat16)
    res_float = residual.astype(f32)
    normed = (
        res_float
        * lax.rsqrt(jnp.mean(res_float * res_float, axis=1, keepdims=True) + epsilon)
        * expert_gain
    ).astype(jnp.bfloat16)
    tok_rows = stream.shape[0]
    width = stream.shape[1]
    top_count = routes.shape[1]
    experts = lax.axis_size("sp")
    capacity = top_count * tok_rows // experts
    flat_ids = routes.reshape(-1)
    onehot = (flat_ids[:, None] == jnp.arange(experts, dtype=jnp.int32)[None, :]).astype(jnp.int32)
    before = jnp.cumsum(onehot, axis=0) - onehot
    rank = jnp.sum(before * onehot, axis=1)
    slots = flat_ids * capacity + rank
    chooser = jnp.any(
        slots.reshape(tok_rows, top_count)[None, :, :]
        == jnp.arange(experts * capacity, dtype=jnp.int32)[:, None, None],
        axis=2,
    ).astype(jnp.bfloat16)
    send_rows = (
        jnp.dot(chooser, normed, preferred_element_type=f32)
        .astype(jnp.bfloat16)
        .reshape(experts, capacity, width)
    )
    gate_w = expert_gate[0]
    up_w = expert_up[0]
    down_w = expert_down[0]
    received = lax.all_to_all(send_rows, "sp", split_axis=0, concat_axis=0, tiled=True)
    flat_recv = received.reshape(-1, width)
    piece = lax.all_gather(flat_recv, "tp", axis=0, tiled=True)
    gate_val = jnp.dot(piece, gate_w, preferred_element_type=f32)
    up_val = jnp.dot(piece, up_w, preferred_element_type=f32)
    hidden = (jax.nn.silu(gate_val) * up_val).astype(jnp.bfloat16)
    summed = lax.psum_scatter(
        jnp.dot(hidden, down_w, preferred_element_type=f32).astype(jnp.bfloat16),
        "tp",
        scatter_dimension=0,
        tiled=True,
    )
    result = summed.reshape(received.shape)
    returned = lax.all_to_all(result, "sp", split_axis=0, concat_axis=0, tiled=True)
    picked = returned.reshape(experts * capacity, width)[slots].reshape(tok_rows, top_count, width)
    expert_sum = jnp.sum(picked.astype(f32) * route_weights[:, :, None], axis=1)
    return (res_float + expert_sum).astype(jnp.bfloat16)


def solution(mesh):
    return jax.shard_map(
        per_device,
        mesh=mesh,
        in_specs=(
            P("tp", "sp"),
            P("tp", "sp"),
            P("tp", None),
            P(),
            P(),
            P(),
            P(("sp", "tp"), None),
            P(("sp", "tp"), None),
            P(("sp", "tp"), None),
            P(),
            P("sp", None, "tp"),
            P("sp", None, "tp"),
            P("sp", "tp", None),
        ),
        out_specs=P(("sp", "tp"), None),
        check_vma=False,
    )
```

profile of v0, /device:TPU:2, one launch (start us, length us, event | category | flops | bytes accessed | tf_op | source)
XLA Modules:
  0.0 225.3 jit_solution(4182957621673231946)
XLA Ops:
  6.5 1.2 multiply_convert_fusion.4
  7.7 0.1 slice.254
  7.8 3.4 %collective-permute-start = (bf16[64,30]{1,0:T(8,128)(2,1)S(1)}, bf16[64,30]{1,0:T(8,128)(2,1)S(1)}, u32[]{:S(2)}, u32[]{:S(2)}) collective-permute-start(bf16[64,30]{1,0:T(8,128)(2,1)S(1)} %slice.254), channel_id=1, source_target_pairs={{0,16},{16,32},{32,48},{48,64},{64,80},{80,96},{96,112},{112,128},... | collective-permute-start | bytes 11528 | tf_op jit(solution)/shard_map/ppermute | solution.py:12
  11.2 1.0 slice_bitcast_fusion.30
  12.2 1.0 slice_bitcast_fusion.29
  13.2 0.8 copy.28
  14.0 0.1 eq.28
  14.1 0.1 fusion.47
  14.2 0.2 reduce_window_sum.11
  14.4 0.2 select_reduce_fusion
  14.6 0.1 reduce_sum.52
  14.7 0.0 collective-permute-done
  14.7 0.1 maximum_convert_fusion
  14.8 2.7 %fusion.10 = bf16[64,1024]{1,0:T(8,128)(2,1)S(1)} fusion(f32[64,1054]{1,0:T(8,128)S(1)} %maximum_convert_fusion, f32[64]{0:T(128)S(1)} %get-tuple-element.36, f32[64]{0:T(128)S(1)} %get-tuple-element.37, f32[64]{0:T(128)S(1)} %get-tuple-element.8, f32[64]{0:T(128)S(1)} %get-tuple-element.9, f32[64]{0:T(128)S(1)} %get-tuple-element.10, ...), kind=kLoop, calls=%fused_computation.23 | loop fusion | flops 4063232 | bytes 8265472 | tf_op jit(solution)/shard_map/convert_element_type | solution.py:44
  17.5 0.0 copy-start.1
  17.5 0.0 copy-start.3
  17.5 0.0 copy-start.4
  17.5 0.2 copy.26
  17.7 0.9 reshape.99
  18.6 8.6 %all-to-all-start = ((bf16[16,2,2048]{2,1,0:T(2,128)(2,1)}), bf16[16,2,2048]{2,1,0:T(2,128)(2,1)S(1)}, u32[]{:S(2)}, u32[]{:S(2)}) async-start(bf16[16,2,2048]{2,1,0:T(2,128)(2,1)} %reshape.99), calls=%async_computation | async-start | bytes 262144 | tf_op jit(solution)/shard_map/all_to_all | solution.py:45
  27.2 0.0 all-gather.2.cloned.1.call-start
  27.3 0.1 copy.30
  27.3 0.1 fusion.48
  27.4 8.4 %all-to-all-done = bf16[16,2,2048]{2,1,0:T(2,128)(2,1)S(1)} async-done(((bf16[16,2,2048]{2,1,0:T(2,128)(2,1)}), bf16[16,2,2048]{2,1,0:T(2,128)(2,1)S(1)}, u32[]{:S(2)}, u32[]{:S(2)}) %all-to-all-start) | async-done | bytes 131104 | tf_op jit(solution)/shard_map/all_to_all | solution.py:45
  35.8 0.2 reshape.100
  36.1 0.2 convert_reduce_fusion
  36.3 0.3 copy.27
  36.6 0.2 reshape.89
  36.8 0.3 fusion.8
  37.1 3.3 %multiply_reduce_fusion.1 = (f32[64]{0:T(128)S(1)}, f32[64,2048]{1,0:T(8,128)S(1)}) fusion(bf16[1024,2048]{1,0:T(8,128)(2,1)} %param.18, f32[1024,64]{0,1:T(8,128)S(1)} %reshape.89, f32[1024]{0:T(1024)S(1)} %copy-done.3, f32[1024]{0:T(1024)S(1)} %copy-done.4, f32[64]{0:T(128)S(1)} %add_rsqrt_fusion.1, f32[64]{0:T(128)S(1)} %broadcast_multiply_fusion.1, ...), kind=kOutput, calls=%fused_computation.20 | convolution fusion | flops 269811648 | bytes 5251840 | tf_op jit(solution)/shard_map/dot_general | solution.py:52
  40.4 0.4 fusion
  40.7 18.1 %all_to_all.23 = bf16[16,8,2048]{2,1,0:T(8,128)(2,1)} all-to-all(bf16[16,8,2048]{2,1,0:T(8,128)(2,1)S(1)} %fusion), channel_id=1, replica_groups=mesh['sp'=16,'tp'=16] {'sp'}, dimensions={0} | all-to-all | bytes 1048576 | tf_op jit(solution)/shard_map/all_to_all | solution.py:85
  58.8 0.0 all-gather.2.cloned.1.call-update
  58.8 0.2 reduce-scatter.2.cloned.1.call-start
  59.1 49.8 %all-gather.2.cloned.1.call-done = bf16[2048,2048]{1,0:T(8,128)(2,1)} async-done(((bf16[128,2048]{1,0:T(8,128)(2,1)}), bf16[2048,2048]{1,0:T(8,128)(2,1)}) %all-gather.2.cloned.1.call-update) | async-done | bytes 8388624 | tf_op jit(solution)/shard_map/all_gather | solution.py:87
  108.8 7.2 %fusion.5 = f32[2048,448]{0,1:T(8,128)S(1)} fusion(bf16[2048,2048]{1,0:T(8,128)(2,1)} %all-gather.2.cloned.1.call-done, bf16[1,2048,448]{1,2,0:T(8,128)(2,1)} %param.23), kind=kOutput, calls=%fused_computation.10 | convolution fusion | flops 3758096384 | bytes 13893632 | tf_op jit(solution)/shard_map/dot_general | solution.py:88
  116.0 4.3 %multiply_convert_fusion = bf16[2048,448]{0,1:T(8,128)(2,1)S(1)} fusion(f32[2048,448]{0,1:T(8,128)S(1)} %fusion.5, bf16[2048,2048]{1,0:T(8,128)(2,1)S(1)} %copy-done.6, bf16[1,2048,448]{1,2,0:T(8,128)(2,1)S(1)} %copy-done.7), kind=kOutput, calls=%fused_computation.2 | convolution fusion | flops 3763601408 | bytes 15728640 | tf_op jit(solution)/shard_map/dot_general | solution.py:89
  120.3 6.9 %convolution_convert_fusion = bf16[2048,2048]{1,0:T(8,128)(2,1)} fusion(bf16[2048,448]{0,1:T(8,128)(2,1)S(1)} %multiply_convert_fusion, bf16[1,448,2048]{2,1,0:T(8,128)(2,1)S(1)} %copy-done), kind=kOutput, calls=%fused_computation.1 | convolution fusion | flops 3762290688 | bytes 12058624 | tf_op jit(solution)/shard_map/dot_general | solution.py:92
  127.2 0.0 reduce-scatter.2.cloned.1.call-update
  127.2 69.5 %reduce-scatter.2.cloned.1.call-done = bf16[128,2048]{1,0:T(8,128)(2,1)} async-done(((bf16[2048,2048]{1,0:T(8,128)(2,1)}), bf16[128,2048]{1,0:T(8,128)(2,1)}) %reduce-scatter.2.cloned.1.call-update) | async-done | bytes 524304 | tf_op jit(solution)/shard_map/reduce_scatter | solution.py:91
  196.8 7.1 %all-to-all-start.2 = ((bf16[16,8,2048]{2,1,0:T(8,128)(2,1)}), bf16[16,8,2048]{2,1,0:T(8,128)(2,1)S(1)}, u32[]{:S(2)}, u32[]{:S(2)}) async-start(bf16[16,8,2048]{2,1,0:T(8,128)(2,1)} %bitcast.100), calls=%async_computation.3 | async-start | bytes 1048576 | tf_op jit(solution)/shard_map/all_to_all | solution.py:98
  203.9 0.1 mul.497
  204.0 0.1 copy.31
  204.2 8.5 %all-to-all-done.2 = bf16[16,8,2048]{2,1,0:T(8,128)(2,1)S(1)} async-done(((bf16[16,8,2048]{2,1,0:T(8,128)(2,1)}), bf16[16,8,2048]{2,1,0:T(8,128)(2,1)S(1)}, u32[]{:S(2)}, u32[]{:S(2)}) %all-to-all-start.2) | async-done | bytes 524320 | tf_op jit(solution)/shard_map/all_to_all | solution.py:98
  212.7 1.7 gather_fusion
  214.4 1.7 reshape.90
  216.1 1.6 multiply_reduce_fusion
  217.7 0.8 add_convert_fusion
  (20 shorter events, 0.1 us)
Async XLA Ops:
  6.5 113.8 %copy-start = (bf16[1,448,2048]{2,1,0:T(8,128)(2,1)S(1)}, bf16[1,448,2048]{2,1,0:T(8,128)(2,1)}, u32[]{:S(2)}) copy-start(bf16[1,448,2048]{2,1,0:T(8,128)(2,1)} %param.25) | copy-start | bytes 5505028
  7.8 6.9 %collective-permute-start = (bf16[64,30]{1,0:T(8,128)(2,1)S(1)}, bf16[64,30]{1,0:T(8,128)(2,1)S(1)}, u32[]{:S(2)}, u32[]{:S(2)}) collective-permute-start(bf16[64,30]{1,0:T(8,128)(2,1)S(1)} %slice.254), channel_id=1, source_target_pairs={{0,16},{16,32},{32,48},{48,64},{64,80},{80,96},{96,112},{112,128},... | collective-permute-start | bytes 11528 | tf_op jit(solution)/shard_map/ppermute | solution.py:12
  17.5 19.5 %copy-start.1 = (bf16[64,2048]{1,0:T(8,128)(2,1)S(1)}, bf16[64,2048]{1,0:T(8,128)(2,1)}, u32[]{:S(2)}) copy-start(bf16[64,2048]{1,0:T(8,128)(2,1)} %param.19) | copy-start | bytes 786436
  17.5 19.5 %copy-start.3 = (f32[1024]{0:T(1024)S(1)}, f32[1024]{0:T(1024)}, u32[]{:S(2)}) copy-start(f32[1024]{0:T(1024)} %param.17) | copy-start | bytes 12292
  17.5 19.5 %copy-start.4 = (f32[1024]{0:T(1024)S(1)}, f32[1024]{0:T(1024)}, u32[]{:S(2)}) copy-start(f32[1024]{0:T(1024)} %param.16) | copy-start | bytes 12292
  18.6 17.2 %all-to-all-start = ((bf16[16,2,2048]{2,1,0:T(2,128)(2,1)}), bf16[16,2,2048]{2,1,0:T(2,128)(2,1)S(1)}, u32[]{:S(2)}, u32[]{:S(2)}) async-start(bf16[16,2,2048]{2,1,0:T(2,128)(2,1)} %reshape.99), calls=%async_computation | async-start | bytes 262144 | tf_op jit(solution)/shard_map/all_to_all | solution.py:45
  27.2 81.6 %all-gather.2.cloned.1.call-start = ((), (), s32[]{:S(2)}) async-start(), calls=%async_computation.4 | async-start | bytes 8912896 | tf_op jit(solution)/shard_map/all_gather | solution.py:87
  36.3 4.1 %copy-start.2 = (f32[2048]{0:T(1024)S(1)}, f32[2048]{0:T(1024)}, u32[]{:S(2)}) copy-start(f32[2048]{0:T(1024)} %param.22) | copy-start | bytes 24580
  58.8 138.0 %reduce-scatter.2.cloned.1.call-start = ((), (), s32[]{:S(2)}) async-start(), calls=%async_computation.5 | async-start | bytes 8912896 | tf_op jit(solution)/shard_map/reduce_scatter | solution.py:91
  108.8 7.2 %copy-start.6 = (bf16[2048,2048]{1,0:T(8,128)(2,1)S(1)}, bf16[2048,2048]{1,0:T(8,128)(2,1)}, u32[]{:S(2)}) copy-start(bf16[2048,2048]{1,0:T(8,128)(2,1)} %all-gather.2.cloned.1.call-done) | copy-start | bytes 25165828
  108.8 7.2 %copy-start.7 = (bf16[1,2048,448]{1,2,0:T(8,128)(2,1)S(1)}, bf16[1,2048,448]{1,2,0:T(8,128)(2,1)}, u32[]{:S(2)}) copy-start(bf16[1,2048,448]{1,2,0:T(8,128)(2,1)} %param.24) | copy-start | bytes 5505028
  127.2 76.8 %copy-start.5 = (f32[64,2]{0,1:T(2,128)S(1)}, f32[64,2]{0,1:T(2,128)}, u32[]{:S(2)}) copy-start(f32[64,2]{0,1:T(2,128)} %param.21) | copy-start | bytes 1540
  196.8 15.9 %all-to-all-start.2 = ((bf16[16,8,2048]{2,1,0:T(8,128)(2,1)}), bf16[16,8,2048]{2,1,0:T(8,128)(2,1)S(1)}, u32[]{:S(2)}, u32[]{:S(2)}) async-start(bf16[16,8,2048]{2,1,0:T(8,128)(2,1)} %bitcast.100), calls=%async_computation.3 | async-start | bytes 1048576 | tf_op jit(solution)/shard_map/all_to_all | solution.py:98
Sparse Core Ops, SparseCore 0:
  59.0 49.8 all-gather.1
  127.4 69.3 reduce-scatter.1
where the time goes:
time: 226 us; the launch traced here: 225 us
  waiting for transfers between devices  136 us (60%)
  matrix products  22 us (10%)
  starting transfers between devices  19.3 us (9%)
  blocking collectives  18.1 us (8%)
  between operations  13.7 us (6%)
  local copies, waits for them, and re-layouts  8.64 us (4%)
  other arithmetic  7.29 us (3%)
    reduce_scatter x1, waiting for transfers between devices, per_device(): lax.psum_scatter(jnp.dot(hidden, down_w, preferred_element_type=f32).asty...  69.5 us
    all_gather x1, waiting for transfers between devices, per_device(): piece = lax.all_gather(flat_recv, 'tp', axis=0, tiled=True)  49.8 us
    all_to_all x1, blocking collectives, per_device(): lax.all_to_all(send_rows, 'sp', split_axis=0, concat_axis=0, tiled=True)  18.1 us
    all_to_all x1, starting transfers between devices, per_device(): lax.all_to_all(conv_out, 'tp', split_axis=1, concat_axis=0, tiled=True)  8.57 us
    all_to_all x1, waiting for transfers between devices, per_device(): lax.all_to_all(result, 'sp', split_axis=0, concat_axis=0, tiled=True)  8.52 us
    all_to_all x1, waiting for transfers between devices, per_device(): lax.all_to_all(conv_out, 'tp', split_axis=1, concat_axis=0, tiled=True)  8.41 us
    dot_general x1, matrix products, per_device(): gate_val = jnp.dot(piece, gate_w, preferred_element_type=f32)  7.17 us
    all_to_all x1, starting transfers between devices, per_device(): lax.all_to_all(result, 'sp', split_axis=0, concat_axis=0, tiled=True)  7.1 us
  transfers between devices with their start and end apart: 5, of which 4 were waited for; matrix products, arithmetic and copies ran while one was open for 2% of the time, Pallas kernels for 0%

commit v1 on v0

v1 whole, which is shorter than its diff:
```python
import functools

import jax
import jax.numpy as jnp
from jax import lax
from jax.experimental import pallas as pl
from jax.experimental.pallas import tpu as pltpu
from jax.sharding import PartitionSpec as P

epsilon = 1e-06
BF16 = jnp.bfloat16
F32 = jnp.float32
MESH = pl.DeviceIdType.MESH


def moe_kernel(
    nsp,
    nz,
    normed_ref,
    resid_ref,
    routes_ref,
    routes_t_ref,
    weights_ref,
    gate_ref,
    up_ref,
    down_ref,
    out_ref,
    gate_w,
    up_w,
    down_w,
    hidden,
    sent,
    x,
    y,
    from_left,
    from_right,
    final,
    returned,
    own_sem,
    mate_send,
    mate_recv,
    disp_send,
    disp_recv,
    ag_send,
    ag_recv,
    rs_send,
    rs_recv,
    ret_send,
    ret_recv,
):
    s = lax.axis_index("sp")
    t = lax.axis_index("tp")
    z = lax.div(t, 2)
    c = lax.rem(t, 2)
    far = nz // 2
    hs = nsp // 2
    right = lax.rem(z + 1, nz) * 2 + c
    left = lax.rem(z + nz - 1, nz) * 2 + c
    mate = z * 2 + 1 - c
    cap = sent.shape[1]
    width = sent.shape[2]
    tokens = normed_ref.shape[0]
    slots = nsp * cap
    shift = cap.bit_length() - 1

    def half(ref, q, h):
        return ref.at[q, pl.ds(h * hs, hs)]

    def remote(src, dst, send, recv, sp, tp):
        return pltpu.make_async_remote_copy(
            src_ref=src,
            dst_ref=dst,
            send_sem=send,
            recv_sem=recv,
            device_id={"sp": sp, "tp": tp},
            device_id_type=MESH,
        )

    pairs = ((gate_ref, gate_w), (up_ref, up_w), (down_ref, down_w))
    for i, (src, dst) in enumerate(pairs):
        pltpu.make_async_copy(src.at[0], dst.at[0], own_sem.at[i]).start()

    barrier = pltpu.get_barrier_semaphore()

    def greet(i, carry):
        pl.semaphore_signal(
            barrier,
            inc=1,
            device_id={"sp": lax.rem(s + i, nsp), "tp": t},
            device_id_type=MESH,
        )
        return carry

    lax.fori_loop(1, nsp, greet, 0)
    for other in (right, left, mate):
        pl.semaphore_signal(barrier, inc=1, device_id={"sp": s, "tp": other}, device_id_type=MESH)

    slot = lax.broadcasted_iota(jnp.int32, (slots, tokens), 0)
    expert = lax.shift_right_logical(slot, shift)
    named = (routes_t_ref[0:1, :] == expert) | (routes_t_ref[1:2, :] == expert)
    before = lax.broadcasted_iota(jnp.int32, (tokens, tokens), 0) < lax.broadcasted_iota(
        jnp.int32, (tokens, tokens), 1
    )
    rank = jnp.dot(
        jnp.where(named, 1.0, 0.0).astype(BF16),
        jnp.where(before, 1.0, 0.0).astype(BF16),
        preferred_element_type=F32,
    )
    pick = named & (rank == (slot & (cap - 1)).astype(F32))
    chosen = jnp.dot(
        jnp.where(pick, 1.0, 0.0).astype(BF16), normed_ref[...], preferred_element_type=F32
    )
    sent[...] = chosen.astype(BF16).reshape(nsp, cap, width)

    pl.semaphore_wait(barrier, nsp + 2)

    def dispatch(i):
        e = lax.rem(s + i, nsp)
        return remote(sent.at[e], x.at[0, s], disp_send.at[i], disp_recv.at[i], e, t)

    def start_dispatch(i, carry):
        dispatch(i).start()
        return carry

    lax.fori_loop(1, nsp, start_dispatch, 0)
    mine = pltpu.make_async_copy(sent.at[s], x.at[0, s], disp_send.at[0])
    mine.start()

    def to_mate(i):
        src, dst = pairs[i]
        return remote(src.at[0], dst.at[1], mate_send.at[i], mate_recv.at[i], s, mate)

    for i in range(3):
        to_mate(i).start()

    def wait_dispatch(i, carry):
        dispatch(i).wait_recv()
        return carry

    lax.fori_loop(1, nsp, wait_dispatch, 0)
    mine.wait()

    def place(way, k):
        return 0 if k == 0 else (2 * k - 1 if way == 0 or k == far else 2 * k)

    def gather(way, k, h):
        return remote(
            half(x, place(way, k), h),
            half(x, place(way, k + 1), h),
            ag_send.at[way, k, h],
            ag_recv.at[place(way, k + 1), h],
            s,
            right if way == 0 else left,
        )

    def goes(way, k, h):
        return k < far - 1 or (k == far - 1 and h == way)

    def ffn(q):
        rows = x[q].reshape(slots, width)
        for b in range(2):
            g = jnp.dot(rows, gate_w[b], preferred_element_type=F32)
            u = jnp.dot(rows, up_w[b], preferred_element_type=F32)
            hidden[b] = (jax.nn.silu(g) * u).astype(BF16)
        tile = min(512, width)

        def columns(j, carry):
            cols = pl.ds(pl.multiple_of(j * tile, tile), tile)
            acc = jnp.dot(hidden[0], down_w[0, :, cols], preferred_element_type=F32)
            acc = acc + jnp.dot(hidden[1], down_w[1, :, cols], preferred_element_type=F32)
            y[q, :, :, cols] = acc.astype(BF16).reshape(nsp, cap, tile)
            return carry

        lax.fori_loop(0, width // tile, columns, 0)

    def ffn_loop(first, last):
        def body(q, carry):
            ffn(q)
            return carry

        lax.fori_loop(first, last, body, 0)

    for h in (0, 1):
        for way in (0, 1):
            hh = h if way == 0 else 1 - h
            if goes(way, 0, hh):
                gather(way, 0, hh).start()
    for i, (src, dst) in enumerate(pairs):
        pltpu.make_async_copy(src.at[0], dst.at[0], own_sem.at[i]).wait()
    for i in range(3):
        to_mate(i).wait_recv()
    ffn_loop(0, 1)
    for k in range(1, far + 1):
        for h in (0, 1):
            for way in (0, 1):
                hh = h if way == 0 else 1 - h
                if goes(way, k - 1, hh):
                    gather(way, k - 1, hh).wait_recv()
                    if goes(way, k, hh):
                        gather(way, k, hh).start()
        ffn_loop(2 * k - 1, min(2 * k + 1, nz))

    def arm(way, r):
        k = far - r
        if k == 0 or k == far:
            return 0 if k == 0 else 2 * far - 1
        return 2 * k if way == 0 else 2 * k - 1

    landed = (from_left, from_right)

    def reduce(way, r, h):
        return remote(
            half(y, arm(way, r), h),
            half(landed[way], r, h),
            rs_send.at[way, r, h],
            rs_recv.at[way, r, h],
            s,
            right if way == 0 else left,
        )

    def moves(way, r, h):
        return r > 0 or h != way

    def add(q, buf, r, h):
        tile = min(512, width)

        def columns(j, carry):
            cols = pl.ds(pl.multiple_of(j * tile, tile), tile)
            rows = pl.ds(h * hs, hs)
            y[q, rows, :, cols] = (
                y[q, rows, :, cols].astype(F32) + buf[r, rows, :, cols].astype(F32)
            ).astype(BF16)
            return carry

        lax.fori_loop(0, width // tile, columns, 0)

    for way in (0, 1):
        reduce(way, 0, 1 - way).start()
    if far > 1:
        for way in (0, 1):
            reduce(way, 1, way).start()
    for r in range(1, far):
        for h in (0, 1):
            for way in (0, 1):
                hh = 1 - h if way == 0 else h
                if r == 1 and hh == way:
                    continue
                reduce(way, r - 1, hh).wait_recv()
                add(arm(way, r), landed[way], r - 1, hh)
                reduce(way, r, hh).start()

    def give_back(i):
        e = lax.rem(s + i, nsp)
        return remote(final.at[e], returned.at[s], ret_send.at[i], ret_recv.at[i], e, t)

    for h in (0, 1):
        rows = pl.ds(h * hs, hs)
        for way in (0, 1):
            if moves(way, far - 1, h):
                reduce(way, far - 1, h).wait_recv()
        tile = min(512, width)

        def columns(j, carry):
            cols = pl.ds(pl.multiple_of(j * tile, tile), tile)
            total = y[0, rows, :, cols].astype(F32)
            for way in (0, 1):
                if moves(way, far - 1, h):
                    total = total + landed[way][far - 1, rows, :, cols].astype(F32)
            final[rows, :, cols] = total.astype(BF16)
            return carry

        lax.fori_loop(0, width // tile, columns, 0)

    def start_back(i, carry):
        give_back(i).start()
        return carry

    lax.fori_loop(1, nsp, start_back, 0)
    kept = pltpu.make_async_copy(final.at[s], returned.at[s], ret_send.at[0])
    kept.start()

    slot = lax.broadcasted_iota(jnp.int32, (tokens, slots), 1)
    expert = lax.shift_right_logical(slot, shift)
    first = routes_ref[:, 0:1] == expert
    second = routes_ref[:, 1:2] == expert
    named = first | second
    before = lax.broadcasted_iota(jnp.int32, (tokens, tokens), 1) < lax.broadcasted_iota(
        jnp.int32, (tokens, tokens), 0
    )
    rank = jnp.dot(
        jnp.where(before, 1.0, 0.0).astype(BF16),
        jnp.where(named, 1.0, 0.0).astype(BF16),
        preferred_element_type=F32,
    )
    pick = named & (rank == (slot & (cap - 1)).astype(F32))
    share = jnp.where(
        pick,
        jnp.where(first, weights_ref[:, 0:1], 0.0) + jnp.where(second, weights_ref[:, 1:2], 0.0),
        0.0,
    )
    high = share.astype(BF16)
    low = (share - high.astype(F32)).astype(BF16)

    def wait_back(i, carry):
        give_back(i).wait_recv()
        return carry

    lax.fori_loop(1, nsp, wait_back, 0)
    kept.wait()
    back = returned[...].reshape(slots, width)
    mixed = jnp.dot(high, back, preferred_element_type=F32)
    mixed = mixed + jnp.dot(low, back, preferred_element_type=F32)
    out_ref[...] = (resid_ref[...].astype(F32) + mixed).astype(BF16)

    def drain(i, carry):
        dispatch(i).wait_send()
        give_back(i).wait_send()
        return carry

    lax.fori_loop(1, nsp, drain, 0)
    for i in range(3):
        to_mate(i).wait_send()
    for way in (0, 1):
        for k in range(far):
            for h in (0, 1):
                if goes(way, k, h):
                    gather(way, k, h).wait_send()
                if moves(way, k, h):
                    reduce(way, k, h).wait_send()


def moe(nsp, nz, normed, residual, routes, route_weights, gate, up, down):
    tokens, width = normed.shape
    hid = gate.shape[2]
    cap = 2 * tokens // nsp
    far = nz // 2
    vmem = pl.BlockSpec(memory_space=pltpu.VMEM)
    hbm = pl.BlockSpec(memory_space=pl.ANY)
    dma = pltpu.SemaphoreType.DMA
    return pl.pallas_call(
        functools.partial(moe_kernel, nsp, nz),
        out_shape=jax.ShapeDtypeStruct((tokens, width), BF16),
        in_specs=[vmem] * 5 + [hbm] * 3,
        out_specs=vmem,
        scratch_shapes=[
            pltpu.VMEM((2, width, hid), BF16),
            pltpu.VMEM((2, width, hid), BF16),
            pltpu.VMEM((2, hid, width), BF16),
            pltpu.VMEM((2, nsp * cap, hid), BF16),
            pltpu.VMEM((nsp, cap, width), BF16),
            pltpu.VMEM((nz, nsp, cap, width), BF16),
            pltpu.VMEM((nz, nsp, cap, width), BF16),
            pltpu.VMEM((far, nsp, cap, width), BF16),
            pltpu.VMEM((far, nsp, cap, width), BF16),
            pltpu.VMEM((nsp, cap, width), BF16),
            pltpu.VMEM((nsp, cap, width), BF16),
            dma((3,)),
            dma((3,)),
            dma((3,)),
            dma((nsp,)),
            dma((nsp,)),
            dma((2, far, 2)),
            dma((nz, 2)),
            dma((2, far, 2)),
            dma((2, far, 2)),
            dma((nsp,)),
            dma((nsp,)),
        ],
        compiler_params=pltpu.CompilerParams(
            collective_id=0, has_side_effects=True, vmem_limit_bytes=60 * 1024 * 1024
        ),
        name="moe",
    )(normed, residual, routes, routes.T, route_weights, gate, up, down)


def shifted(value, axis, steps):
    count = lax.axis_size(axis)
    initial, last = (max(0, -steps), min(count, count - steps))
    return lax.ppermute(value, axis, [(source, source + steps) for source in range(initial, last)])


def per_device(
    conv_value,
    conv_gate,
    conv_taps,
    norm_gain,
    norm_bias,
    out_weight,
    stream,
    routes,
    route_weights,
    expert_gain,
    expert_gate,
    expert_up,
    expert_down,
):
    f32 = jnp.float32
    local_ch = conv_value.shape[0]
    run_len = conv_value.shape[1]
    kernel_len = conv_taps.shape[1]
    gated_input = (conv_value.astype(f32) * jax.nn.sigmoid(conv_gate.astype(f32))).astype(
        jnp.bfloat16
    )
    left_rim = shifted(gated_input[:, run_len - (kernel_len - 1) :], "sp", 1)
    padded = jnp.concatenate([left_rim, gated_input], axis=1).astype(f32)
    conv_sum = jnp.zeros((local_ch, run_len), f32)
    for offset in range(kernel_len):
        conv_sum = (
            conv_sum + conv_taps[:, offset : offset + 1] * padded[:, offset : offset + run_len]
        )
    conv_out = conv_sum.astype(jnp.bfloat16)
    whole_conv = lax.all_to_all(conv_out, "tp", split_axis=1, concat_axis=0, tiled=True).astype(f32)
    center = jnp.mean(whole_conv, axis=0, keepdims=True)
    spread = jnp.mean((whole_conv - center) ** 2, axis=0, keepdims=True)
    scaled = (whole_conv - center) * lax.rsqrt(spread + epsilon) * norm_gain[:, None] + norm_bias[
        :, None
    ]
    token_major = jax.nn.silu(scaled).astype(jnp.bfloat16)
    projected = lax.dot_general(
        token_major, out_weight, (((0,), (0,)), ((), ())), preferred_element_type=f32
    )
    residual = (stream.astype(f32) + projected).astype(jnp.bfloat16)
    res_float = residual.astype(f32)
    normed = (
        res_float
        * lax.rsqrt(jnp.mean(res_float * res_float, axis=1, keepdims=True) + epsilon)
        * expert_gain
    ).astype(jnp.bfloat16)
    return moe(
        lax.axis_size("sp"),
        lax.axis_size("tp") // 2,
        normed,
        residual,
        routes,
        route_weights,
        expert_gate,
        expert_up,
        expert_down,
    )


def solution(mesh):
    return jax.shard_map(
        per_device,
        mesh=mesh,
        in_specs=(
            P("tp", "sp"),
            P("tp", "sp"),
            P("tp", None),
            P(),
            P(),
            P(),
            P(("sp", "tp"), None),
            P(("sp", "tp"), None),
            P(("sp", "tp"), None),
            P(),
            P("sp", None, "tp"),
            P("sp", None, "tp"),
            P("sp", "tp", None),
        ),
        out_specs=P(("sp", "tp"), None),
        check_vma=False,
    )
```

time: 226 us -> 145 us (0.64)
  waiting for transfers between devices: 136 us -> 1.25 us
  Pallas kernels: 0 us -> 109 us
  matrix products: 22 us -> 3.28 us
  blocking collectives: 18.1 us -> 0 us
  between operations: 13.7 us -> 0.19 us
  starting transfers between devices: 19.3 us -> 12 us
  local copies, waits for them, and re-layouts: 8.64 us -> 13.1 us
    pallas_call x0 -> x1, Pallas kernels: none -> 109 us  [moe(): pl.pallas_call(functools.partial(moe_kernel, nsp, nz), out_shape=jax.Shap...]
    reduce_scatter x1 -> x0, waiting for transfers between devices: 69.5 us -> none  [per_device(): lax.psum_scatter(jnp.dot(hidden, down_w, preferred_element_type=f32).asty...]
    all_gather x1 -> x0, waiting for transfers between devices: 49.8 us -> none  [per_device(): piece = lax.all_gather(flat_recv, 'tp', axis=0, tiled=True)]
    dot_general x4 -> x0, matrix products: 18.7 us -> none  [the longest x1 7.17 us: per_device(): gate_val = jnp.dot(piece, gate_w, preferred_element_type=f32)]
    all_to_all x1 -> x0, blocking collectives: 18.1 us -> none  [per_device(): lax.all_to_all(send_rows, 'sp', split_axis=0, concat_axis=0, tiled=True)]
    all_to_all x1 -> x0, waiting for transfers between devices: 8.52 us -> none  [per_device(): lax.all_to_all(result, 'sp', split_axis=0, concat_axis=0, tiled=True)]
    unnamed x20 -> x23, local copies, waits for them, and re-layouts: 2.02 us -> 10.4 us
    all_to_all x1, waiting for transfers between devices: 8.41 us -> 0.99 us  [per_device(): lax.all_to_all(conv_out, 'tp', split_axis=1, concat_axis=0, tiled=True)]
  transfers between devices with their start and end apart: 5 -> 2, of which waited for: 4 -> 2; matrix products, arithmetic and copies ran while one was open for 2% -> 7% of each run, Pallas kernels for 0% -> 0%
where the time goes in v1:
time: 145 us; the launch traced here: 144 us
  Pallas kernels  109 us (75%)
  local copies, waits for them, and re-layouts  13.1 us (9%)
  starting transfers between devices  12 us (8%)
  other arithmetic  5.11 us (4%)
  matrix products  3.28 us (2%)
    pallas_call x1, Pallas kernels, moe(): pl.pallas_call(functools.partial(moe_kernel, nsp, nz), out_shape=jax.Shap...  109 us
    unnamed x23, local copies, waits for them, and re-layouts  10.4 us
    all_to_all x1, starting transfers between devices, per_device(): lax.all_to_all(conv_out, 'tp', split_axis=1, concat_axis=0, tiled=True)  8.58 us
    ppermute x1, starting transfers between devices, shifted(): lax.ppermute(value, axis, [(source, source + steps) for source in range(i...  3.39 us
    dot_general x1, matrix products, per_device(): lax.dot_general(token_major, out_weight, (((0,), (0,)), ((), ())), prefer...  3.28 us
  transfers between devices with their start and end apart: 2, of which 2 were waited for; matrix products, arithmetic and copies ran while one was open for 7% of the time, Pallas kernels for 0%

profile of v1, /device:TPU:2, one launch (start us, length us, event | category | flops | bytes accessed | tf_op | source)
XLA Modules:
  0.0 144.0 jit_solution(13362183402570075607)
XLA Ops:
  0.0 1.0 multiply_convert_fusion.1
  1.0 0.1 slice.252
  1.1 3.4 %collective-permute-start = (bf16[64,30]{1,0:T(8,128)(2,1)S(1)}, bf16[64,30]{1,0:T(8,128)(2,1)S(1)}, u32[]{:S(2)}, u32[]{:S(2)}) collective-permute-start(bf16[64,30]{1,0:T(8,128)(2,1)S(1)} %slice.252), channel_id=1, source_target_pairs={{0,16},{16,32},{32,48},{48,64},{64,80},{80,96},{96,112},{112,128},... | collective-permute-start | bytes 11528 | tf_op jit(solution)/shard_map/ppermute | solution.py:379
  4.5 1.0 slice_bitcast_fusion.30
  5.5 1.0 slice_bitcast_fusion.29
  6.5 0.3 collective-permute-done
  6.7 0.1 maximum_convert_fusion
  6.9 0.0 copy-start.7
  6.9 0.0 copy-start.4
  6.9 0.0 copy-start.1
  6.9 2.7 %fusion.7 = bf16[64,1024]{1,0:T(8,128)(2,1)S(1)} fusion(f32[64,1054]{1,0:T(8,128)S(1)} %maximum_convert_fusion, f32[64]{0:T(128)S(1)} %get-tuple-element.34, f32[64]{0:T(128)S(1)} %get-tuple-element.35, f32[64]{0:T(128)S(1)} %get-tuple-element.6, f32[64]{0:T(128)S(1)} %get-tuple-element.7, f32[64]{0:T(128)S(1)} %get-tuple-element.8, ...), kind=kLoop, calls=%fused_computation.14 | loop fusion | flops 4063232 | bytes 8265472 | tf_op jit(solution)/shard_map/convert_element_type | solution.py:411
  9.6 0.2 copy.23
  9.7 0.9 reshape.34
  10.6 8.6 %all-to-all-start = ((bf16[16,2,2048]{2,1,0:T(2,128)(2,1)}), bf16[16,2,2048]{2,1,0:T(2,128)(2,1)S(1)}, u32[]{:S(2)}, u32[]{:S(2)}) async-start(bf16[16,2,2048]{2,1,0:T(2,128)(2,1)} %reshape.34), calls=%async_computation | async-start | bytes 262144 | tf_op jit(solution)/shard_map/all_to_all | solution.py:412
  19.2 0.0 copy-done.7
  19.2 0.7 copy.26.weights_ref
  19.9 0.0 copy-done.4
  19.9 0.7 copy.25.routes_ref
  20.6 0.0 copy-done.1
  20.6 2.4 %copy.27.gate_ref = bf16[1,2048,448]{2,1,0:T(8,128)(2,1)} copy(bf16[1,2048,448]{1,2,0:T(8,128)(2,1)S(1)} %copy-done.1) | data formatting | bytes 3670016 | tf_op args[10]
  23.1 3.8 %copy.28.up_ref = bf16[1,2048,448]{2,1,0:T(8,128)(2,1)} copy(bf16[1,2048,448]{1,2,0:T(8,128)(2,1)} %param.24) | data formatting | bytes 3670016 | tf_op args[11]
  26.9 0.0 copy-start.2
  26.9 0.0 copy-start.5
  26.9 0.0 copy-start.6
  26.9 1.0 all-to-all-done
  27.9 0.2 reshape.35
  28.1 0.2 convert_reduce_fusion
  28.3 0.3 fusion.5
  28.6 0.3 copy.24
  28.9 0.2 reshape.33
  29.1 0.0 copy-done.2
  29.1 0.0 copy-done.5
  29.1 0.0 copy-done.6
  29.1 0.0 copy-start.3
  29.1 3.3 %fusion.1 = (f32[64]{0:T(128)S(1)}, bf16[64,2048]{1,0:T(8,128)(2,1)S(1)}) fusion(bf16[1024,2048]{1,0:T(8,128)(2,1)} %param.18, f32[1024,64]{0,1:T(8,128)S(1)} %reshape.33, f32[1024]{0:T(1024)S(1)} %copy-done.5, f32[1024]{0:T(1024)S(1)} %copy-done.6, f32[64]{0:T(128)S(1)} %add_rsqrt_fusion.1, f32[64]{0:T(128)S(1)} %broadcast_multiply_fusion, ...), kind=kOutput, calls=%fused_computation.7 | convolution fusion | flops 269811648 | bytes 4989696 | tf_op jit(solution)/shard_map/dot_general | solution.py:419
  32.4 0.0 copy-start
  32.4 0.0 copy-done.3
  32.4 0.8 fusion.3.normed_ref
  33.2 0.0 copy-done
  33.3 109.1 %moe.1 = bf16[64,2048]{1,0:T(8,128)(2,1)} custom-call(bf16[64,2048]{1,0:T(8,128)(2,1)} %fusion.3.normed_ref, bf16[64,2048]{1,0:T(8,128)(2,1)} %copy-done, s32[64,2]{1,0:T(8,128)} %copy.25.routes_ref, s32[2,64]{1,0:T(2,128)} %bitcast.75, f32[64,2]{1,0:T(8,128)} %copy.26.weights_ref, bf16[1,2048,448]{2,1,0:T(8,128)(2,1)} %copy.27.gate_ref, ...), custom_call_target="tpu_custom_call" | custom-call | tf_op jit(solution)/shard_map/moe/pallas_call | solution.py:340
  142.4 1.7 %copy.30 = bf16[64,2048]{1,0:T(8,128)(2,1)} copy(bf16[64,2048]{1,0:T(8,128)(2,1)} %moe.1) | data formatting | bytes 524288
  (4 shorter events, 0.1 us)
Async XLA Ops:
  1.1 5.6 %collective-permute-start = (bf16[64,30]{1,0:T(8,128)(2,1)S(1)}, bf16[64,30]{1,0:T(8,128)(2,1)S(1)}, u32[]{:S(2)}, u32[]{:S(2)}) collective-permute-start(bf16[64,30]{1,0:T(8,128)(2,1)S(1)} %slice.252), channel_id=1, source_target_pairs={{0,16},{16,32},{32,48},{48,64},{64,80},{80,96},{96,112},{112,128},... | collective-permute-start | bytes 11528 | tf_op jit(solution)/shard_map/ppermute | solution.py:379
  6.9 12.4 %copy-start.7 = (f32[64,2]{0,1:T(2,128)S(1)}, f32[64,2]{0,1:T(2,128)}, u32[]{:S(2)}) copy-start(f32[64,2]{0,1:T(2,128)} %param.21) | copy-start | bytes 1540
  6.9 13.1 %copy-start.4 = (s32[64,2]{0,1:T(2,128)S(1)}, s32[64,2]{0,1:T(2,128)}, u32[]{:S(2)}) copy-start(s32[64,2]{0,1:T(2,128)} %param.20) | copy-start | bytes 1540
  6.9 13.8 %copy-start.1 = (bf16[1,2048,448]{1,2,0:T(8,128)(2,1)S(1)}, bf16[1,2048,448]{1,2,0:T(8,128)(2,1)}, u32[]{:S(2)}) copy-start(bf16[1,2048,448]{1,2,0:T(8,128)(2,1)} %param.23) | copy-start | bytes 5505028
  10.6 17.2 %all-to-all-start = ((bf16[16,2,2048]{2,1,0:T(2,128)(2,1)}), bf16[16,2,2048]{2,1,0:T(2,128)(2,1)S(1)}, u32[]{:S(2)}, u32[]{:S(2)}) async-start(bf16[16,2,2048]{2,1,0:T(2,128)(2,1)} %reshape.34), calls=%async_computation | async-start | bytes 262144 | tf_op jit(solution)/shard_map/all_to_all | solution.py:412
  26.9 2.2 %copy-start.2 = (bf16[64,2048]{1,0:T(8,128)(2,1)S(1)}, bf16[64,2048]{1,0:T(8,128)(2,1)}, u32[]{:S(2)}) copy-start(bf16[64,2048]{1,0:T(8,128)(2,1)} %param.19) | copy-start | bytes 786436
  26.9 2.2 %copy-start.5 = (f32[1024]{0:T(1024)S(1)}, f32[1024]{0:T(1024)}, u32[]{:S(2)}) copy-start(f32[1024]{0:T(1024)} %param.17) | copy-start | bytes 12292
  26.9 2.2 %copy-start.6 = (f32[1024]{0:T(1024)S(1)}, f32[1024]{0:T(1024)}, u32[]{:S(2)}) copy-start(f32[1024]{0:T(1024)} %param.16) | copy-start | bytes 12292
  29.1 3.3 %copy-start.3 = (f32[2048]{0:T(1024)S(1)}, f32[2048]{0:T(1024)}, u32[]{:S(2)}) copy-start(f32[2048]{0:T(1024)} %param.22) | copy-start | bytes 24580
  32.4 0.9 copy-start

commit v2 on v1

--- a/solution.py
+++ b/solution.py
@@ -11,20 +11,35 @@
 BF16 = jnp.bfloat16
 F32 = jnp.float32
 MESH = pl.DeviceIdType.MESH
-
-
-def moe_kernel(
+by_row = (((1,), (1,)), ((), ()))
+
+
+def kernel(
     nsp,
     nz,
-    normed_ref,
-    resid_ref,
+    value_ref,
+    gating_ref,
+    taps_ref,
+    affine_ref,
+    out_w_ref,
+    stream_ref,
     routes_ref,
-    routes_t_ref,
     weights_ref,
+    gain_ref,
     gate_ref,
     up_ref,
     down_ref,
     out_ref,
+    gated,
+    spread_taps,
+    edge,
+    rim,
+    conv_out,
+    conv_in,
+    act,
+    out_w,
+    stream,
+    resid,
     gate_w,
     up_w,
     down_w,
@@ -36,6 +51,11 @@
     from_right,
     final,
     returned,
+    in_sem,
+    rim_send,
+    rim_recv,
+    conv_send,
+    conv_recv,
     own_sem,
     mate_send,
     mate_recv,
@@ -59,9 +79,16 @@
     mate = z * 2 + 1 - c
     cap = sent.shape[1]
     width = sent.shape[2]
-    tokens = normed_ref.shape[0]
+    tokens = routes_ref.shape[1]
     slots = nsp * cap
     shift = cap.bit_length() - 1
+    local_ch, run_len = value_ref.shape
+    taps = taps_ref.shape[0]
+    lanes = 2 * tokens
+    sub = local_ch // 2
+    group = act.shape[2]
+    channels = 2 * group
+    tile = min(512, width)
 
     def half(ref, q, h):
         return ref.at[q, pl.ds(h * hs, hs)]
@@ -80,9 +107,17 @@
     for i, (src, dst) in enumerate(pairs):
         pltpu.make_async_copy(src.at[0], dst.at[0], own_sem.at[i]).start()
 
+    loads = [
+        pltpu.make_async_copy(out_w_ref.at[:, 0], out_w.at[0], in_sem.at[0]),
+        pltpu.make_async_copy(out_w_ref.at[:, 1], out_w.at[1], in_sem.at[1]),
+        pltpu.make_async_copy(stream_ref, stream, in_sem.at[2]),
+    ]
+    for load in loads:
+        load.start()
+
     barrier = pltpu.get_barrier_semaphore()
 
-    def greet(i, carry):
+    def greet_sp(i, carry):
         pl.semaphore_signal(
             barrier,
             inc=1,
@@ -91,13 +126,142 @@
         )
         return carry
 
-    lax.fori_loop(1, nsp, greet, 0)
-    for other in (right, left, mate):
-        pl.semaphore_signal(barrier, inc=1, device_id={"sp": s, "tp": other}, device_id_type=MESH)
+    def greet_tp(i, carry):
+        pl.semaphore_signal(
+            barrier,
+            inc=1,
+            device_id={"sp": s, "tp": lax.rem(t + i, 2 * nz)},
+            device_id_type=MESH,
+        )
+        return carry
+
+    lax.fori_loop(1, nsp, greet_sp, 0)
+    lax.fori_loop(1, 2 * nz, greet_tp, 0)
+
+    for p in range(nz - 1, -1, -1):
+        cols = slice(p * lanes, (p + 1) * lanes)
+        product = value_ref[:, cols].astype(F32) * jax.nn.sigmoid(gating_ref[:, cols].astype(F32))
+        if p == nz - 1:
+            edge[...] = product.astype(BF16)
+        gated[p + 1] = product.astype(BF16).astype(F32)
+    by_channel = taps_ref[...].T
+    for j in range(taps):
+        spread_taps[j] = jnp.broadcast_to(by_channel[:, j : j + 1], (local_ch, lanes))
+
+    pl.semaphore_wait(barrier, nsp + 2 * nz - 2)
+
+    def to_next():
+        return remote(edge, rim, rim_send.at[0], rim_recv.at[0], lax.rem(s + 1, nsp), t)
+
+    @pl.when(s < nsp - 1)
+    def _():
+        to_next().start()
+
+    def to_owner(p, core):
+        return remote(
+            conv_out.at[p, core], conv_in.at[t], conv_send.at[p, core], conv_recv.at[t], s, 2 * p + core
+        )
+
+    def stays(p, core):
+        return pltpu.make_async_copy(conv_out.at[p, core], conv_in.at[t], conv_recv.at[t])
+
+    lane = lax.broadcasted_iota(jnp.int32, (local_ch, lanes), 1)
+    low_lanes = lax.broadcasted_iota(jnp.int32, (sub, lanes), 1) < tokens
+
+    def conv_tile(i, carry):
+        p = nz - 1 - i
+
+        @pl.when(p == 0)
+        def _():
+            @pl.when(s > 0)
+            def _():
+                to_next().wait_recv()
+                gated[0] = rim[...].astype(F32)
+
+            @pl.when(s == 0)
+            def _():
+                gated[0] = jnp.zeros((local_ch, lanes), F32)
+
+        here, before = gated[p + 1], gated[p]
+        total = spread_taps[taps - 1] * here
+        for d in range(1, taps):
+            window = pltpu.roll(jnp.where(lane >= lanes - d, before, here), d, 1)
+            total = total + spread_taps[taps - 1 - d] * window
+        top, bottom = total[:sub], total[sub:]
+        conv_out[p, 0] = jnp.where(low_lanes, top, pltpu.roll(bottom, tokens, 1)).astype(BF16)
+        conv_out[p, 1] = jnp.where(low_lanes, pltpu.roll(top, tokens, 1), bottom).astype(BF16)
+        for core in (0, 1):
+
+            @pl.when(2 * p + core != t)
+            def _():
+                to_owner(p, core).start()
+
+            @pl.when(2 * p + core == t)
+            def _():
+                stays(p, core).start()
+
+        return carry
+
+    lax.fori_loop(0, nz, conv_tile, 0)
+
+    def to_mate(i):
+        src, dst = pairs[i]
+        return remote(src.at[0], dst.at[1], mate_send.at[i], mate_recv.at[i], s, mate)
+
+    for i in range(3):
+        to_mate(i).start()
+
+    def wait_conv(i, carry):
+        @pl.when(i != t)
+        def _():
+            remote(
+                conv_out.at[0, 0], conv_in.at[i], conv_send.at[0, 0], conv_recv.at[i], s, i
+            ).wait_recv()
+
+        @pl.when(i == t)
+        def _():
+            stays(z, 0).wait()
+
+        return carry
+
+    lax.fori_loop(0, 2 * nz, wait_conv, 0)
+
+    def over_channels(value):
+        part = jnp.sum(value, axis=0, keepdims=True)
+        return (part + pltpu.roll(part, tokens, 1)) * (1.0 / channels)
+
+    whole = conv_in[...].reshape(group, lanes).astype(F32)
+    deviation = whole - over_channels(whole)
+    spread = over_channels(deviation * deviation)
+    scaled = (deviation * lax.rsqrt(spread + epsilon)).T
+    for h in (0, 1):
+        part = scaled[h * tokens : (h + 1) * tokens]
+        act[h] = jax.nn.silu(part * affine_ref[h : h + 1, :] + affine_ref[2 + h : 3 + h, :]).astype(
+            BF16
+        )
+    for load in loads:
+        load.wait()
+
+    def project(j, squares):
+        cols = pl.ds(pl.multiple_of(j * tile, tile), tile)
+        acc = stream[:, cols].astype(F32)
+        for h in (0, 1):
+            acc = acc + jnp.dot(
+                act[h], out_w[h, :, :, cols].reshape(group, tile), preferred_element_type=F32
+            )
+        rounded = acc.astype(BF16)
+        resid[:, cols] = rounded
+        wide = rounded.astype(F32)
+        return squares + jnp.sum(wide * wide, axis=1, keepdims=True)
+
+    squares = lax.fori_loop(0, width // tile, project, jnp.zeros((tokens, 1), F32))
+    scale = lax.rsqrt(squares * (1.0 / width) + epsilon)
 
     slot = lax.broadcasted_iota(jnp.int32, (slots, tokens), 0)
     expert = lax.shift_right_logical(slot, shift)
-    named = (routes_t_ref[0:1, :] == expert) | (routes_t_ref[1:2, :] == expert)
+    first = routes_ref[0:1, :] == expert
+    second = routes_ref[1:2, :] == expert
+    named = first | second
     before = lax.broadcasted_iota(jnp.int32, (tokens, tokens), 0) < lax.broadcasted_iota(
         jnp.int32, (tokens, tokens), 1
     )
@@ -107,12 +271,16 @@
         preferred_element_type=F32,
     )
     pick = named & (rank == (slot & (cap - 1)).astype(F32))
-    chosen = jnp.dot(
-        jnp.where(pick, 1.0, 0.0).astype(BF16), normed_ref[...], preferred_element_type=F32
-    )
-    sent[...] = chosen.astype(BF16).reshape(nsp, cap, width)
-
-    pl.semaphore_wait(barrier, nsp + 2)
+    chooser = jnp.where(pick, 1.0, 0.0).astype(BF16)
+
+    def fill(j, carry):
+        cols = pl.ds(pl.multiple_of(j * tile, tile), tile)
+        normed = (resid[:, cols].astype(F32) * scale * gain_ref[:, cols]).astype(BF16)
+        chosen = jnp.dot(chooser, normed, preferred_element_type=F32)
+        sent[:, :, cols] = chosen.astype(BF16).reshape(nsp, cap, tile)
+        return carry
+
+    lax.fori_loop(0, width // tile, fill, 0)
 
     def dispatch(i):
         e = lax.rem(s + i, nsp)
@@ -125,13 +293,6 @@
     lax.fori_loop(1, nsp, start_dispatch, 0)
     mine = pltpu.make_async_copy(sent.at[s], x.at[0, s], disp_send.at[0])
     mine.start()
-
-    def to_mate(i):
-        src, dst = pairs[i]
-        return remote(src.at[0], dst.at[1], mate_send.at[i], mate_recv.at[i], s, mate)
-
-    for i in range(3):
-        to_mate(i).start()
 
     def wait_dispatch(i, carry):
         dispatch(i).wait_recv()
@@ -159,10 +320,9 @@
     def ffn(q):
         rows = x[q].reshape(slots, width)
         for b in range(2):
-            g = jnp.dot(rows, gate_w[b], preferred_element_type=F32)
-            u = jnp.dot(rows, up_w[b], preferred_element_type=F32)
+            g = lax.dot_general(rows, gate_w[b], by_row, preferred_element_type=F32)
+            u = lax.dot_general(rows, up_w[b], by_row, preferred_element_type=F32)
             hidden[b] = (jax.nn.silu(g) * u).astype(BF16)
-        tile = min(512, width)
 
         def columns(j, carry):
             cols = pl.ds(pl.multiple_of(j * tile, tile), tile)
@@ -222,7 +382,6 @@
         return r > 0 or h != way
 
     def add(q, buf, r, h):
-        tile = min(512, width)
 
         def columns(j, carry):
             cols = pl.ds(pl.multiple_of(j * tile, tile), tile)
@@ -258,7 +417,6 @@
         for way in (0, 1):
             if moves(way, far - 1, h):
                 reduce(way, far - 1, h).wait_recv()
-        tile = min(512, width)
 
         def columns(j, carry):
             cols = pl.ds(pl.multiple_of(j * tile, tile), tile)
@@ -279,25 +437,11 @@
     kept = pltpu.make_async_copy(final.at[s], returned.at[s], ret_send.at[0])
     kept.start()
 
-    slot = lax.broadcasted_iota(jnp.int32, (tokens, slots), 1)
-    expert = lax.shift_right_logical(slot, shift)
-    first = routes_ref[:, 0:1] == expert
-    second = routes_ref[:, 1:2] == expert
-    named = first | second
-    before = lax.broadcasted_iota(jnp.int32, (tokens, tokens), 1) < lax.broadcasted_iota(
-        jnp.int32, (tokens, tokens), 0
-    )
-    rank = jnp.dot(
-        jnp.where(before, 1.0, 0.0).astype(BF16),
-        jnp.where(named, 1.0, 0.0).astype(BF16),
-        preferred_element_type=F32,
-    )
-    pick = named & (rank == (slot & (cap - 1)).astype(F32))
     share = jnp.where(
         pick,
-        jnp.where(first, weights_ref[:, 0:1], 0.0) + jnp.where(second, weights_ref[:, 1:2], 0.0),
+        jnp.where(first, weights_ref[0:1, :], 0.0) + jnp.where(second, weights_ref[1:2, :], 0.0),
         0.0,
-    )
+    ).T
     high = share.astype(BF16)
     low = (share - high.astype(F32)).astype(BF16)
 
@@ -310,7 +454,22 @@
     back = returned[...].reshape(slots, width)
     mixed = jnp.dot(high, back, preferred_element_type=F32)
     mixed = mixed + jnp.dot(low, back, preferred_element_type=F32)
-    out_ref[...] = (resid_ref[...].astype(F32) + mixed).astype(BF16)
+    out_ref[...] = (resid[...].astype(F32) + mixed).astype(BF16)
+
+    @pl.when(s < nsp - 1)
+    def _():
+        to_next().wait_send()
+
+    def drain_conv(p, carry):
+        for core in (0, 1):
+
+            @pl.when(2 * p + core != t)
+            def _():
+                to_owner(p, core).wait_send()
+
+        return carry
+
+    lax.fori_loop(0, nz, drain_conv, 0)
 
     def drain(i, carry):
         dispatch(i).wait_send()
@@ -329,22 +488,54 @@
                     reduce(way, k, h).wait_send()
 
 
-def moe(nsp, nz, normed, residual, routes, route_weights, gate, up, down):
-    tokens, width = normed.shape
-    hid = gate.shape[2]
+def per_device(
+    conv_value,
+    conv_gate,
+    conv_taps,
+    norm_gain,
+    norm_bias,
+    out_weight,
+    stream,
+    routes,
+    route_weights,
+    expert_gain,
+    expert_gate,
+    expert_up,
+    expert_down,
+):
+    nsp, ntp = lax.axis_size("sp"), lax.axis_size("tp")
+    nz = ntp // 2
+    tokens, width = stream.shape
+    local_ch, taps = conv_taps.shape
+    sub = local_ch // 2
+    hid = expert_gate.shape[2]
     cap = 2 * tokens // nsp
     far = nz // 2
+    lanes = 2 * tokens
+    group = ntp * sub
+    affine = jnp.stack([norm_gain, norm_bias]).reshape(2, ntp, 2, sub)
+    affine = affine.transpose(0, 2, 1, 3).reshape(4, group)
     vmem = pl.BlockSpec(memory_space=pltpu.VMEM)
     hbm = pl.BlockSpec(memory_space=pl.ANY)
     dma = pltpu.SemaphoreType.DMA
     return pl.pallas_call(
-        functools.partial(moe_kernel, nsp, nz),
+        functools.partial(kernel, nsp, nz),
         out_shape=jax.ShapeDtypeStruct((tokens, width), BF16),
-        in_specs=[vmem] * 5 + [hbm] * 3,
+        in_specs=[vmem] * 4 + [hbm] * 2 + [vmem] * 3 + [hbm] * 3,
         out_specs=vmem,
         scratch_shapes=[
-            pltpu.VMEM((2, width, hid), BF16),
-            pltpu.VMEM((2, width, hid), BF16),
+            pltpu.VMEM((nz + 1, local_ch, lanes), F32),
+            pltpu.VMEM((taps, local_ch, lanes), F32),
+            pltpu.VMEM((local_ch, lanes), BF16),
+            pltpu.VMEM((local_ch, lanes), BF16),
+            pltpu.VMEM((nz, 2, sub, lanes), BF16),
+            pltpu.VMEM((ntp, sub, lanes), BF16),
+            pltpu.VMEM((2, tokens, group), BF16),
+            pltpu.VMEM((2, ntp, sub, width), BF16),
+            pltpu.VMEM((tokens, width), BF16),
+            pltpu.VMEM((tokens, width), BF16),
+            pltpu.VMEM((2, hid, width), BF16),
+            pltpu.VMEM((2, hid, width), BF16),
             pltpu.VMEM((2, hid, width), BF16),
             pltpu.VMEM((2, nsp * cap, hid), BF16),
             pltpu.VMEM((nsp, cap, width), BF16),
@@ -354,6 +545,11 @@
             pltpu.VMEM((far, nsp, cap, width), BF16),
             pltpu.VMEM((nsp, cap, width), BF16),
             pltpu.VMEM((nsp, cap, width), BF16),
+            dma((3,)),
+            dma((1,)),
+            dma((1,)),
+            dma((nz, 2)),
+            dma((ntp,)),
             dma((3,)),
             dma((3,)),
             dma((3,)),
@@ -369,72 +565,19 @@
         compiler_params=pltpu.CompilerParams(
             collective_id=0, has_side_effects=True, vmem_limit_bytes=60 * 1024 * 1024
         ),
-        name="moe",
-    )(normed, residual, routes, routes.T, route_weights, gate, up, down)
-
-
-def shifted(value, axis, steps):
-    count = lax.axis_size(axis)
-    initial, last = (max(0, -steps), min(count, count - steps))
-    return lax.ppermute(value, axis, [(source, source + steps) for source in range(initial, last)])
-
-
-def per_device(
-    conv_value,
-    conv_gate,
-    conv_taps,
-    norm_gain,
-    norm_bias,
-    out_weight,
-    stream,
-    routes,
-    route_weights,
-    expert_gain,
-    expert_gate,
-    expert_up,
-    expert_down,
-):
-    f32 = jnp.float32
-    local_ch = conv_value.shape[0]
-    run_len = conv_value.shape[1]
-    kernel_len = conv_taps.shape[1]
-    gated_input = (conv_value.astype(f32) * jax.nn.sigmoid(conv_gate.astype(f32))).astype(
-        jnp.bfloat16
-    )
-    left_rim = shifted(gated_input[:, run_len - (kernel_len - 1) :], "sp", 1)
-    padded = jnp.concatenate([left_rim, gated_input], axis=1).astype(f32)
-    conv_sum = jnp.zeros((local_ch, run_len), f32)
-    for offset in range(kernel_len):
-        conv_sum = (
-            conv_sum + conv_taps[:, offset : offset + 1] * padded[:, offset : offset + run_len]
-        )
-    conv_out = conv_sum.astype(jnp.bfloat16)
-    whole_conv = lax.all_to_all(conv_out, "tp", split_axis=1, concat_axis=0, tiled=True).astype(f32)
-    center = jnp.mean(whole_conv, axis=0, keepdims=True)
-    spread = jnp.mean((whole_conv - center) ** 2, axis=0, keepdims=True)
-    scaled = (whole_conv - center) * lax.rsqrt(spread + epsilon) * norm_gain[:, None] + norm_bias[
-        :, None
-    ]
-    token_major = jax.nn.silu(scaled).astype(jnp.bfloat16)
-    projected = lax.dot_general(
-        token_major, out_weight, (((0,), (0,)), ((), ())), preferred_element_type=f32
-    )
-    residual = (stream.astype(f32) + projected).astype(jnp.bfloat16)
-    res_float = residual.astype(f32)
-    normed = (
-        res_float
-        * lax.rsqrt(jnp.mean(res_float * res_float, axis=1, keepdims=True) + epsilon)
-        * expert_gain
-    ).astype(jnp.bfloat16)
-    return moe(
-        lax.axis_size("sp"),
-        lax.axis_size("tp") // 2,
-        normed,
-        residual,
-        routes,
-        route_weights,
-        expert_gate,
-        expert_up,
+        name="block",
+    )(
+        conv_value,
+        conv_gate,
+        conv_taps.T,
+        affine,
+        out_weight.reshape(ntp, 2, sub, width),
+        stream,
+        routes.T,
+        route_weights.T,
+        expert_gain[None, :],
+        expert_gate.swapaxes(1, 2),
+        expert_up.swapaxes(1, 2),
         expert_down,
     )
 

time: 145 us -> 131 us (0.903)
  Pallas kernels: 109 us -> 127 us
  starting transfers between devices: 12 us -> 0 us
  local copies, waits for them, and re-layouts: 13.1 us -> 3.89 us
  other arithmetic: 5.11 us -> 0.02 us
  matrix products: 3.28 us -> 0 us
    pallas_call x1, Pallas kernels: 109 us -> 127 us  [per_device(): pl.pallas_call(functools.partial(kernel, nsp, nz), out_shape=jax.ShapeDty...]
    unnamed x23 -> x1, local copies, waits for them, and re-layouts: 10.4 us -> 1.67 us
    all_to_all x1 -> x0, starting transfers between devices: 8.58 us -> none  [per_device(): lax.all_to_all(conv_out, 'tp', split_axis=1, concat_axis=0, tiled=True)]
    convert_element_type x5 -> x0, other arithmetic: 4.69 us -> none  [the longest x1 2.66 us: per_device(): conv_out = conv_sum.astype(jnp.bfloat16)]
    ppermute x1 -> x0, starting transfers between devices: 3.39 us -> none  [shifted(): lax.ppermute(value, axis, [(source, source + steps) for source in range(i...]
    dot_general x1 -> x0, matrix products: 3.28 us -> none  [per_device(): lax.dot_general(token_major, out_weight, (((0,), (0,)), ((), ())), prefer...]
    mul x2 -> x0, local copies, waits for them, and re-layouts: 1.96 us -> none  [per_device(): conv_taps[:, offset:offset + 1] * padded[:, offset:offset + run_len]]
    another operation x0 -> x2, local copies, waits for them, and re-layouts: none -> 1.53 us  [per_device(): affine = jnp.stack([norm_gain, norm_bias]).reshape(2, ntp, 2, sub)]
  transfers between devices with their start and end apart: 2 -> 0, of which waited for: 2 -> 0; matrix products, arithmetic and copies ran while one was open for 7% -> 0% of each run, Pallas kernels for 0% -> 0%
where the time goes in v2:
time: 131 us
  Pallas kernels  127 us (97%)
  local copies, waits for them, and re-layouts  3.89 us (3%)
    pallas_call x1, Pallas kernels, per_device(): pl.pallas_call(functools.partial(kernel, nsp, nz), out_shape=jax.ShapeDty...  127 us

profile of v2, /device:TPU:2, one launch (start us, length us, event | category | flops | bytes accessed | tf_op | source)
XLA Modules:
  0.0 130.5 jit_solution(13984804510307015581)
XLA Ops:
  0.0 0.8 stack.9
  0.8 0.8 stack.10
  1.6 0.7 reshape.11.affine_ref
  2.3 126.6 %block.1 = bf16[64,2048]{1,0:T(8,128)(2,1)} custom-call(bf16[64,1024]{1,0:T(8,128)(2,1)} %value_ref.1, bf16[64,1024]{1,0:T(8,128)(2,1)} %gating_ref.1, f32[31,64]{1,0:T(8,128)} %bitcast.14, f32[4,512]{1,0:T(4,128)} %reshape.11.affine_ref, bf16[16,2,32,2048]{3,2,1,0:T(8,128)(2,1)} %bitcast.11, bf16[64,2048]{1,0:T(8,128)(2,1)} %stream_ref.1, ...), custom_call_target="tpu_custom_call" | custom-call | tf_op jit(solution)/shard_map/block/pallas_call | solution.py:521
  128.8 1.7 %copy.16 = bf16[64,2048]{1,0:T(8,128)(2,1)} copy(bf16[64,2048]{1,0:T(8,128)(2,1)} %block.1) | data formatting | bytes 524288
  (2 shorter events, 0.0 us)

commit v3 on v2

v3 whole, which is shorter than its diff:
```python
import functools

import jax
import jax.numpy as jnp
from jax import lax
from jax.experimental import pallas as pl
from jax.experimental.pallas import tpu as pltpu
from jax.sharding import PartitionSpec as P

epsilon = 1e-06
BF16 = jnp.bfloat16
F32 = jnp.float32
MESH = pl.DeviceIdType.MESH
by_row = (((1,), (1,)), ((), ()))


def kernel(
    nsp,
    nz,
    early,
    value_ref,
    gating_ref,
    taps_ref,
    norm_gain_ref,
    norm_bias_ref,
    out_w_ref,
    stream_ref,
    routes_ref,
    weights_ref,
    gain_ref,
    gate_ref,
    up_ref,
    down_ref,
    out_ref,
    gated,
    spread_taps,
    edge,
    rim,
    conv_out,
    conv_in,
    act,
    out_w,
    stream,
    resid,
    gate_w,
    up_w,
    down_w,
    hidden,
    info,
    tokens_at,
    sent,
    x,
    y,
    back_at,
    sums,
    from_left,
    from_right,
    sums_left,
    sums_right,
    final,
    returned,
    in_sem,
    rim_send,
    rim_recv,
    conv_send,
    conv_recv,
    own_sem,
    mate_send,
    mate_recv,
    info_send,
    info_recv,
    disp_send,
    disp_recv,
    plane_send,
    plane_recv,
    tok_send,
    tok_recv,
    ag_send,
    ag_recv,
    rs_send,
    rs_recv,
    sum_send,
    sum_recv,
    back_send,
    back_recv,
    ret_send,
    ret_recv,
):
    s = lax.axis_index("sp")
    t = lax.axis_index("tp")
    z = lax.div(t, 2)
    c = lax.rem(t, 2)
    far = nz // 2
    hs = nsp // 2
    right = lax.rem(z + 1, nz) * 2 + c
    left = lax.rem(z + nz - 1, nz) * 2 + c
    mate = z * 2 + 1 - c
    cap = sent.shape[2]
    width = sent.shape[3]
    tokens = routes_ref.shape[1]
    slots = nsp * cap
    shift = cap.bit_length() - 1
    local_ch, run_len = value_ref.shape
    taps = taps_ref.shape[0]
    lanes = 2 * tokens
    sub = local_ch // 2
    group = act.shape[2]
    channels = 2 * group
    tile = min(512, early)
    ht = tokens // 2
    late = pl.ds(early, width - early)
    ahead = pl.ds(0, early)

    def half(ref, q, h):
        return ref.at[q, pl.ds(h * hs, hs), :, late]

    def column_loop(first, last, body):
        def step(j, carry):
            body(pl.ds(pl.multiple_of(j * tile, tile), tile))
            return carry

        lax.fori_loop(first // tile, last // tile, step, 0)

    def remote(src, dst, send, recv, sp, tp):
        return pltpu.make_async_remote_copy(
            src_ref=src,
            dst_ref=dst,
            send_sem=send,
            recv_sem=recv,
            device_id={"sp": sp, "tp": tp},
            device_id_type=MESH,
        )

    pairs = ((gate_ref, gate_w), (up_ref, up_w), (down_ref, down_w))
    for i, (src, dst) in enumerate(pairs):
        pltpu.make_async_copy(src.at[0], dst.at[0], own_sem.at[i]).start()

    loads = [
        pltpu.make_async_copy(out_w_ref.at[:, 0], out_w.at[0], in_sem.at[0]),
        pltpu.make_async_copy(out_w_ref.at[:, 1], out_w.at[1], in_sem.at[1]),
        pltpu.make_async_copy(stream_ref, stream, in_sem.at[2]),
    ]
    for load in loads:
        load.start()

    barrier = pltpu.get_barrier_semaphore()

    def greet_sp(i, carry):
        pl.semaphore_signal(
            barrier,
            inc=1,
            device_id={"sp": lax.rem(s + i, nsp), "tp": t},
            device_id_type=MESH,
        )
        return carry

    def greet_tp(i, carry):
        pl.semaphore_signal(
            barrier,
            inc=1,
            device_id={"sp": s, "tp": lax.rem(t + i, 2 * nz)},
            device_id_type=MESH,
        )
        return carry

    lax.fori_loop(1, nsp, greet_sp, 0)
    lax.fori_loop(1, 2 * nz, greet_tp, 0)

    for p in range(nz - 1, -1, -1):
        cols = slice(p * lanes, (p + 1) * lanes)
        product = value_ref[:, cols].astype(F32) * jax.nn.sigmoid(gating_ref[:, cols].astype(F32))
        if p == nz - 1:
            edge[...] = product.astype(BF16)
        gated[p + 1] = product.astype(BF16).astype(F32)
    by_channel = taps_ref[...].T
    for j in range(taps):
        spread_taps[j] = jnp.broadcast_to(by_channel[:, j : j + 1], (local_ch, lanes))

    slot = lax.broadcasted_iota(jnp.int32, (slots, tokens), 0)
    expert = lax.shift_right_logical(slot, shift)
    first = routes_ref[0:1, :] == expert
    second = routes_ref[1:2, :] == expert
    named = first | second
    before = lax.broadcasted_iota(jnp.int32, (tokens, tokens), 0) < lax.broadcasted_iota(
        jnp.int32, (tokens, tokens), 1
    )
    rank = jnp.dot(
        jnp.where(named, 1.0, 0.0).astype(BF16),
        jnp.where(before, 1.0, 0.0).astype(BF16),
        preferred_element_type=F32,
    )
    pick = named & (rank == (slot & (cap - 1)).astype(F32))
    number = slot.astype(F32)
    info[0] = jnp.zeros((8, lanes), F32)
    for i, hit in enumerate((first, second)):
        info[0, i : i + 1, :tokens] = jnp.sum(
            jnp.where(hit & pick, number, 0.0), axis=0, keepdims=True
        )
        info[0, 2 + i : 3 + i, :tokens] = weights_ref[i : i + 1, :]

    def regroup(ref, h):
        return jnp.concatenate(
            [ref[:, pl.ds((2 * i + h) * sub, sub)] for i in range(2 * nz)], axis=1
        )

    affine = [(regroup(norm_gain_ref, h), regroup(norm_bias_ref, h)) for h in (0, 1)]

    pl.semaphore_wait(barrier, nsp + 2 * nz - 2)

    def to_next():
        return remote(edge, rim, rim_send.at[0], rim_recv.at[0], lax.rem(s + 1, nsp), t)

    @pl.when(s < nsp - 1)
    def _():
        to_next().start()

    def tell(i):
        q = jnp.where(i <= far, 2 * i - 1, 2 * (nz - i))
        return remote(
            info.at[0], info.at[q], info_send.at[i], info_recv.at[q], s, lax.rem(z + i, nz) * 2 + c
        )

    def start_tell(i, carry):
        tell(i).start()
        return carry

    lax.fori_loop(1, nz, start_tell, 0)

    def to_owner(p, core):
        return remote(
            conv_out.at[p, core], conv_in.at[t], conv_send.at[p, core], conv_recv.at[t], s, 2 * p + core
        )

    def stays(p, core):
        return pltpu.make_async_copy(conv_out.at[p, core], conv_in.at[t], conv_recv.at[t])

    lane = lax.broadcasted_iota(jnp.int32, (local_ch, lanes), 1)
    low_lanes = lax.broadcasted_iota(jnp.int32, (sub, lanes), 1) < tokens

    def conv_tile(i, carry):
        p = nz - 1 - i

        @pl.when(p == 0)
        def _():
            @pl.when(s > 0)
            def _():
                to_next().wait_recv()
                gated[0] = rim[...].astype(F32)

            @pl.when(s == 0)
            def _():
                gated[0] = jnp.zeros((local_ch, lanes), F32)

        here, before = gated[p + 1], gated[p]
        total = spread_taps[taps - 1] * here
        for d in range(1, taps):
            window = pltpu.roll(jnp.where(lane >= lanes - d, before, here), d, 1)
            total = total + spread_taps[taps - 1 - d] * window
        top, bottom = total[:sub], total[sub:]
        conv_out[p, 0] = jnp.where(low_lanes, top, pltpu.roll(bottom, tokens, 1)).astype(BF16)
        conv_out[p, 1] = jnp.where(low_lanes, pltpu.roll(top, tokens, 1), bottom).astype(BF16)
        for core in (0, 1):

            @pl.when(2 * p + core != t)
            def _():
                to_owner(p, core).start()

            @pl.when(2 * p + core == t)
            def _():
                stays(p, core).start()

        return carry

    lax.fori_loop(0, nz, conv_tile, 0)

    def to_mate(i):
        src, dst = pairs[i]
        return remote(src.at[0], dst.at[1], mate_send.at[i], mate_recv.at[i], s, mate)

    for i in range(3):
        to_mate(i).start()

    def wait_conv(i, carry):
        @pl.when(i != t)
        def _():
            remote(
                conv_out.at[0, 0], conv_in.at[i], conv_send.at[0, 0], conv_recv.at[i], s, i
            ).wait_recv()

        @pl.when(i == t)
        def _():
            stays(z, 0).wait()

        return carry

    lax.fori_loop(0, 2 * nz, wait_conv, 0)

    def over_channels(value):
        part = jnp.sum(value, axis=0, keepdims=True)
        return (part + pltpu.roll(part, tokens, 1)) * (1.0 / channels)

    whole = conv_in[...].reshape(group, lanes).astype(F32)
    deviation = whole - over_channels(whole)
    spread = over_channels(deviation * deviation)
    scaled = (deviation * lax.rsqrt(spread + epsilon)).T
    for h in (0, 1):
        part = scaled[h * tokens : (h + 1) * tokens]
        act[h] = jax.nn.silu(part * affine[h][0] + affine[h][1]).astype(
            BF16
        )
    for load in loads:
        load.wait()

    def project(j, squares):
        cols = pl.ds(pl.multiple_of(j * tile, tile), tile)
        acc = stream[:, cols].astype(F32)
        for h in (0, 1):
            acc = acc + jnp.dot(
                act[h], out_w[h, :, :, cols].reshape(group, tile), preferred_element_type=F32
            )
        rounded = acc.astype(BF16)
        resid[:, cols] = rounded
        wide = rounded.astype(F32)
        return squares + jnp.sum(wide * wide, axis=1, keepdims=True)

    squares = lax.fori_loop(0, width // tile, project, jnp.zeros((tokens, 1), F32))
    scale = lax.rsqrt(squares * (1.0 / width) + epsilon)

    def place(way, k):
        return 0 if k == 0 else (2 * k - 1 if way == 0 or k == far else 2 * k)

    def goes(way, k, h):
        return k < far - 1 or (k == far - 1 and h == way)

    def spread(way, k, h):
        return remote(
            tokens_at.at[place(way, k), h],
            tokens_at.at[place(way, k + 1), h],
            tok_send.at[way, k, h],
            tok_recv.at[place(way, k + 1), h],
            s,
            right if way == 0 else left,
        )

    def start_hop(copy, k):
        for h in (0, 1):
            for way in (0, 1):
                hh = h if way == 0 else 1 - h
                if goes(way, k, hh):
                    copy(way, k, hh).start()

    def pass_on(copy, k):
        for h in (0, 1):
            for way in (0, 1):
                hh = h if way == 0 else 1 - h
                if goes(way, k - 1, hh):
                    copy(way, k - 1, hh).wait_recv()
                    if goes(way, k, hh):
                        copy(way, k, hh).start()

    def normalize(cols):
        return (resid[:, cols].astype(F32) * scale * gain_ref[:, cols]).astype(BF16)

    def set_tokens(cols):
        tokens_at[0, :, :, cols] = normalize(cols).reshape(2, ht, tile)

    column_loop(0, early, set_tokens)
    start_hop(spread, 0)

    slot_of = lax.broadcasted_iota(jnp.int32, (slots, tokens), 0).astype(F32)

    def hits(q, i):
        return slot_of == info[q, i : i + 1, :tokens]

    def chooser(q):
        return jnp.where(hits(q, 0) | hits(q, 1), 1.0, 0.0).astype(BF16)

    def weigher(q):
        share = jnp.where(hits(q, 0), info[q, 2:3, :tokens], 0.0) + jnp.where(
            hits(q, 1), info[q, 3:4, :tokens], 0.0
        )
        share = share.T
        high = share.astype(BF16)
        return high, (share - high.astype(F32)).astype(BF16)

    def choose(q, rows, cols, pick):
        chosen = jnp.dot(pick, rows, preferred_element_type=F32)
        sent[q, :, :, cols] = chosen.astype(BF16).reshape(nsp, cap, tile)

    def over_plane(src, dst, q, cols, send, recv):
        def copy(i):
            e = lax.rem(s + i, nsp)
            return remote(src.at[q, e, :, cols], dst.at[q, s, :, cols], send, recv, e, t)

        def begin(i, carry):
            copy(i).start()
            return carry

        lax.fori_loop(1, nsp, begin, 0)
        pltpu.make_async_copy(src.at[q, s, :, cols], dst.at[q, s, :, cols], recv).start()

    def all_in(dst, q, cols, recv):
        pltpu.make_async_copy(dst.at[q, :, :, cols], dst.at[q, :, :, cols], recv).wait()

    def all_out(src, q, cols, send):
        block = src.at[q, pl.ds(0, nsp - 1), :, cols]
        pltpu.make_async_copy(block, block, send).wait()

    own_pick = chooser(0)
    column_loop(early, width, lambda cols: choose(0, normalize(cols), cols, own_pick))
    over_plane(sent, x, 0, late, disp_send.at[0], disp_recv.at[0])
    column_loop(
        0, early, lambda cols: choose(0, tokens_at[0, :, :, cols].reshape(tokens, tile), cols, own_pick)
    )
    over_plane(sent, x, 0, ahead, plane_send.at[0], plane_recv.at[0])

    def tell_in(q):
        pltpu.make_async_copy(info.at[q], info.at[q], info_recv.at[q]).wait()

    def select(q):
        tell_in(q)
        pick = chooser(q)
        column_loop(
            0, early, lambda cols: choose(q, tokens_at[q, :, :, cols].reshape(tokens, tile), cols, pick)
        )
        over_plane(sent, x, q, ahead, plane_send.at[q], plane_recv.at[q])

    def q_loop(first, last, f):
        def body(q, carry):
            f(q)
            return carry

        lax.fori_loop(first, last, body, 0)

    pass_on(spread, 1)
    q_loop(1, min(3, nz), select)
    all_in(x, 0, late, disp_recv.at[0])

    def gather(way, k, h):
        return remote(
            half(x, place(way, k), h),
            half(x, place(way, k + 1), h),
            ag_send.at[way, k, h],
            ag_recv.at[place(way, k + 1), h],
            s,
            right if way == 0 else left,
        )

    def ffn(q):
        rows = x[q].reshape(slots, width)
        for b in range(2):
            g = lax.dot_general(rows, gate_w[b], by_row, preferred_element_type=F32)
            u = lax.dot_general(rows, up_w[b], by_row, preferred_element_type=F32)
            hidden[b] = (jax.nn.silu(g) * u).astype(BF16)

        def columns(j, carry):
            cols = pl.ds(pl.multiple_of(j * tile, tile), tile)
            acc = jnp.dot(hidden[0], down_w[0, :, cols], preferred_element_type=F32)
            acc = acc + jnp.dot(hidden[1], down_w[1, :, cols], preferred_element_type=F32)
            y[q, :, :, cols] = acc.astype(BF16).reshape(nsp, cap, tile)
            return carry

        lax.fori_loop(0, width // tile, columns, 0)

    def experts(q):
        all_in(x, q, ahead, plane_recv.at[q])
        ffn(q)
        over_plane(y, back_at, q, ahead, back_send.at[q], back_recv.at[q])

    start_hop(gather, 0)
    for k in range(2, far + 1):
        pass_on(spread, k)
        q_loop(2 * k - 1, min(2 * k + 1, nz), select)
    for i, (src, dst) in enumerate(pairs):
        pltpu.make_async_copy(src.at[0], dst.at[0], own_sem.at[i]).wait()
    for i in range(3):
        to_mate(i).wait_recv()
    q_loop(0, 1, experts)
    for k in range(1, far + 1):
        pass_on(gather, k)
        q_loop(2 * k - 1, min(2 * k + 1, nz), experts)

    def arm(way, r):
        k = far - r
        if k == 0 or k == far:
            return 0 if k == 0 else 2 * far - 1
        return 2 * k if way == 0 else 2 * k - 1

    landed = (from_left, from_right)

    def reduce(way, r, h):
        return remote(
            half(y, arm(way, r), h),
            half(landed[way], r, h),
            rs_send.at[way, r, h],
            rs_recv.at[way, r, h],
            s,
            right if way == 0 else left,
        )

    def moves(way, r, h):
        return r > 0 or h != way

    def add(q, buf, r, h):
        rows = pl.ds(h * hs, hs)

        def body(cols):
            y[q, rows, :, cols] = (
                y[q, rows, :, cols].astype(F32) + buf[r, rows, :, cols].astype(F32)
            ).astype(BF16)

        column_loop(early, width, body)

    sums_landed = (sums_left, sums_right)

    def reduce_sums(way, r, h):
        return remote(
            sums.at[arm(way, r), h],
            sums_landed[way].at[r, h],
            sum_send.at[way, r, h],
            sum_recv.at[way, r, h],
            s,
            right if way == 0 else left,
        )

    def add_sums(q, buf, r, h):
        sums[q, h] = (sums[q, h].astype(F32) + buf[r, h].astype(F32)).astype(BF16)

    def combine(q):
        all_in(back_at, q, ahead, back_recv.at[q])
        high, low = weigher(q)

        def body(cols):
            rows = back_at[q, :, :, cols].reshape(slots, tile)
            mixed = jnp.dot(high, rows, preferred_element_type=F32)
            mixed = mixed + jnp.dot(low, rows, preferred_element_type=F32)
            sums[q, :, :, cols] = mixed.astype(BF16).reshape(2, ht, tile)

        column_loop(0, early, body)

    def open_arms(copy):
        for way in (0, 1):
            copy(way, 0, 1 - way).start()

    def second_halves(copy):
        if far > 1:
            for way in (0, 1):
                copy(way, 1, way).start()

    def advance(copy, plus, bufs, r):
        for h in (0, 1):
            for way in (0, 1):
                hh = 1 - h if way == 0 else h
                if r == 1 and hh == way:
                    continue
                copy(way, r - 1, hh).wait_recv()
                plus(arm(way, r), bufs[way], r - 1, hh)
                copy(way, r, hh).start()

    open_arms(reduce)
    second_halves(reduce)
    q_loop(nz - 1, nz, combine)
    open_arms(reduce_sums)
    if far > 1:
        q_loop(nz - 3, nz - 1, combine)
        second_halves(reduce_sums)
    for r in range(1, far):
        advance(reduce, add, landed, r)
        if r + 1 < far:
            q_loop(nz - 3 - 2 * r, nz - 1 - 2 * r, combine)
        advance(reduce_sums, add_sums, sums_landed, r)
    q_loop(0, 1, combine)

    for h in (0, 1):
        rows = pl.ds(h * hs, hs)
        for way in (0, 1):
            if moves(way, far - 1, h):
                reduce(way, far - 1, h).wait_recv()

        def finish(cols):
            total = y[0, rows, :, cols].astype(F32)
            for way in (0, 1):
                if moves(way, far - 1, h):
                    total = total + landed[way][far - 1, rows, :, cols].astype(F32)
            final[0, rows, :, cols] = total.astype(BF16)

        column_loop(early, width, finish)

    over_plane(final, returned, 0, late, ret_send.at[0], ret_recv.at[0])

    for h in (0, 1):
        rows = pl.ds(h * ht, ht)
        for way in (0, 1):
            if moves(way, far - 1, h):
                reduce_sums(way, far - 1, h).wait_recv()

        def finish_sums(cols):
            total = resid[rows, cols].astype(F32) + sums[0, h, :, cols].astype(F32)
            for way in (0, 1):
                if moves(way, far - 1, h):
                    total = total + sums_landed[way][far - 1, h, :, cols].astype(F32)
            out_ref[rows, cols] = total.astype(BF16)

        column_loop(0, early, finish_sums)

    high, low = weigher(0)
    all_in(returned, 0, late, ret_recv.at[0])

    def finish_late(cols):
        rows = returned[0, :, :, cols].reshape(slots, tile)
        mixed = jnp.dot(high, rows, preferred_element_type=F32)
        mixed = mixed + jnp.dot(low, rows, preferred_element_type=F32)
        out_ref[:, cols] = (resid[:, cols].astype(F32) + mixed).astype(BF16)

    column_loop(early, width, finish_late)

    @pl.when(s < nsp - 1)
    def _():
        to_next().wait_send()

    def drain_conv(p, carry):
        for core in (0, 1):

            @pl.when(2 * p + core != t)
            def _():
                to_owner(p, core).wait_send()

        return carry

    lax.fori_loop(0, nz, drain_conv, 0)

    def drain_tell(i, carry):
        tell(i).wait_send()
        return carry

    lax.fori_loop(1, nz, drain_tell, 0)
    all_out(sent, 0, late, disp_send.at[0])
    all_out(final, 0, late, ret_send.at[0])

    def drain_plane(q):
        all_out(sent, q, ahead, plane_send.at[q])
        all_out(y, q, ahead, back_send.at[q])

    q_loop(0, nz, drain_plane)
    for i in range(3):
        to_mate(i).wait_send()
    for way in (0, 1):
        for k in range(far):
            for h in (0, 1):
                if goes(way, k, h):
                    gather(way, k, h).wait_send()
                    spread(way, k, h).wait_send()
                if moves(way, k, h):
                    reduce(way, k, h).wait_send()
                    reduce_sums(way, k, h).wait_send()


def per_device(
    conv_value,
    conv_gate,
    conv_taps,
    norm_gain,
    norm_bias,
    out_weight,
    stream,
    routes,
    route_weights,
    expert_gain,
    expert_gate,
    expert_up,
    expert_down,
):
    nsp, ntp = lax.axis_size("sp"), lax.axis_size("tp")
    nz = ntp // 2
    tokens, width = stream.shape
    local_ch, taps = conv_taps.shape
    sub = local_ch // 2
    hid = expert_gate.shape[2]
    cap = 2 * tokens // nsp
    far = nz // 2
    lanes = 2 * tokens
    group = ntp * sub
    early = width // 2
    vmem = pl.BlockSpec(memory_space=pltpu.VMEM)
    hbm = pl.BlockSpec(memory_space=pl.ANY)
    dma = pltpu.SemaphoreType.DMA
    return pl.pallas_call(
        functools.partial(kernel, nsp, nz, early),
        out_shape=jax.ShapeDtypeStruct((tokens, width), BF16),
        in_specs=[vmem] * 5 + [hbm] * 2 + [vmem] * 3 + [hbm] * 3,
        out_specs=vmem,
        scratch_shapes=[
            pltpu.VMEM((nz + 1, local_ch, lanes), F32),
            pltpu.VMEM((taps, local_ch, lanes), F32),
            pltpu.VMEM((local_ch, lanes), BF16),
            pltpu.VMEM((local_ch, lanes), BF16),
            pltpu.VMEM((nz, 2, sub, lanes), BF16),
            pltpu.VMEM((ntp, sub, lanes), BF16),
            pltpu.VMEM((2, tokens, group), BF16),
            pltpu.VMEM((2, ntp, sub, width), BF16),
            pltpu.VMEM((tokens, width), BF16),
            pltpu.VMEM((tokens, width), BF16),
            pltpu.VMEM((2, hid, width), BF16),
            pltpu.VMEM((2, hid, width), BF16),
            pltpu.VMEM((2, hid, width), BF16),
            pltpu.VMEM((2, nsp * cap, hid), BF16),
            pltpu.VMEM((nz, 8, lanes), F32),
            pltpu.VMEM((nz, 2, tokens // 2, early), BF16),
            pltpu.VMEM((nz, nsp, cap, width), BF16),
            pltpu.VMEM((nz, nsp, cap, width), BF16),
            pltpu.VMEM((nz, nsp, cap, width), BF16),
            pltpu.VMEM((nz, nsp, cap, early), BF16),
            pltpu.VMEM((nz, 2, tokens // 2, early), BF16),
            pltpu.VMEM((far, nsp, cap, width), BF16),
            pltpu.VMEM((far, nsp, cap, width), BF16),
            pltpu.VMEM((far, 2, tokens // 2, early), BF16),
            pltpu.VMEM((far, 2, tokens // 2, early), BF16),
            pltpu.VMEM((1, nsp, cap, width), BF16),
            pltpu.VMEM((1, nsp, cap, width), BF16),
            dma((3,)),
            dma((1,)),
            dma((1,)),
            dma((nz, 2)),
            dma((ntp,)),
            dma((3,)),
            dma((3,)),
            dma((3,)),
            dma((nz,)),
            dma((nz,)),
            dma((1,)),
            dma((1,)),
            dma((nz,)),
            dma((nz,)),
            dma((2, far, 2)),
            dma((nz, 2)),
            dma((2, far, 2)),
            dma((nz, 2)),
            dma((2, far, 2)),
            dma((2, far, 2)),
            dma((2, far, 2)),
            dma((2, far, 2)),
            dma((nz,)),
            dma((nz,)),
            dma((1,)),
            dma((1,)),
        ],
        compiler_params=pltpu.CompilerParams(
            collective_id=0, has_side_effects=True, vmem_limit_bytes=60 * 1024 * 1024
        ),
        name="block",
    )(
        conv_value,
        conv_gate,
        conv_taps.T,
        norm_gain[None, :],
        norm_bias[None, :],
        out_weight.reshape(ntp, 2, sub, width),
        stream,
        routes.T,
        route_weights.T,
        expert_gain[None, :],
        expert_gate.swapaxes(1, 2),
        expert_up.swapaxes(1, 2),
        expert_down,
    )


def solution(mesh):
    return jax.shard_map(
        per_device,
        mesh=mesh,
        in_specs=(
            P("tp", "sp"),
            P("tp", "sp"),
            P("tp", None),
            P(),
            P(),
            P(),
            P(("sp", "tp"), None),
            P(("sp", "tp"), None),
            P(("sp", "tp"), None),
            P(),
            P("sp", None, "tp"),
            P("sp", None, "tp"),
            P("sp", "tp", None),
        ),
        out_specs=P(("sp", "tp"), None),
        check_vma=False,
    )
```

time: 131 us -> 111 us (0.85)
  Pallas kernels: 127 us -> 109 us
  local copies, waits for them, and re-layouts: 3.89 us -> 1.67 us
    pallas_call x1, Pallas kernels: 127 us -> 109 us  [per_device(): pl.pallas_call(functools.partial(kernel, nsp, nz, early), out_shape=jax.S...]
    another operation x2 -> x0, local copies, waits for them, and re-layouts: 1.53 us -> none  [per_device(): affine = jnp.stack([norm_gain, norm_bias]).reshape(2, ntp, 2, sub)]
where the time goes in v3:
time: 111 us
  Pallas kernels  109 us (98%)
  local copies, waits for them, and re-layouts  1.67 us (2%)
    pallas_call x1, Pallas kernels, per_device(): pl.pallas_call(functools.partial(kernel, nsp, nz, early), out_shape=jax.S...  109 us

profile of v3, /device:TPU:2, one launch (start us, length us, event | category | flops | bytes accessed | tf_op | source)
XLA Modules:
  0.0 111.0 jit_solution(1439362167676357312)
XLA Ops:
  0.0 109.3 %block.1 = bf16[64,2048]{1,0:T(8,128)(2,1)} custom-call(bf16[64,1024]{1,0:T(8,128)(2,1)} %value_ref.1, bf16[64,1024]{1,0:T(8,128)(2,1)} %gating_ref.1, f32[31,64]{1,0:T(8,128)} %bitcast.12, f32[1,1024]{1,0:T(1,128)} %bitcast.14, f32[1,1024]{1,0:T(1,128)} %bitcast.15, bf16[16,2,32,2048]{3,2,1,0:T(8,128)(2,1)} %bitcast.9, bf16[64,2048]{1,0:T(8,128)(2,1)} %stream_ref.1, ...), custom_call_target="tpu_custom_call" | custom-call | tf_op jit(solution)/shard_map/block/pallas_call | solution.py:687
  109.4 1.7 %copy.15 = bf16[64,2048]{1,0:T(8,128)(2,1)} copy(bf16[64,2048]{1,0:T(8,128)(2,1)} %block.1) | data formatting | bytes 524288

commit v4 on v3

--- a/solution.py
+++ b/solution.py
@@ -107,6 +107,7 @@
     group = act.shape[2]
     channels = 2 * group
     tile = min(512, early)
+    wide = min(512, width)
     ht = tokens // 2
     late = pl.ds(early, width - early)
     ahead = pl.ds(0, early)
@@ -131,10 +132,6 @@
             device_id_type=MESH,
         )
 
-    pairs = ((gate_ref, gate_w), (up_ref, up_w), (down_ref, down_w))
-    for i, (src, dst) in enumerate(pairs):
-        pltpu.make_async_copy(src.at[0], dst.at[0], own_sem.at[i]).start()
-
     loads = [
         pltpu.make_async_copy(out_w_ref.at[:, 0], out_w.at[0], in_sem.at[0]),
         pltpu.make_async_copy(out_w_ref.at[:, 1], out_w.at[1], in_sem.at[1]),
@@ -142,6 +139,9 @@
     ]
     for load in loads:
         load.start()
+    pairs = ((gate_ref, gate_w), (up_ref, up_w), (down_ref, down_w))
+    for i, (src, dst) in enumerate(pairs):
+        pltpu.make_async_copy(src.at[0], dst.at[0], own_sem.at[i]).start()
 
     barrier = pltpu.get_barrier_semaphore()
 
@@ -446,26 +446,59 @@
             right if way == 0 else left,
         )
 
-    def ffn(q):
-        rows = x[q].reshape(slots, width)
+    def ffn(q, n):
+        rows = x[pl.ds(q, n)].reshape(n * slots, width)
+        filled = pl.ds(0, n * slots)
         for b in range(2):
             g = lax.dot_general(rows, gate_w[b], by_row, preferred_element_type=F32)
             u = lax.dot_general(rows, up_w[b], by_row, preferred_element_type=F32)
-            hidden[b] = (jax.nn.silu(g) * u).astype(BF16)
+            hidden[b, filled] = (jax.nn.silu(g) * u).astype(BF16)
 
         def columns(j, carry):
-            cols = pl.ds(pl.multiple_of(j * tile, tile), tile)
-            acc = jnp.dot(hidden[0], down_w[0, :, cols], preferred_element_type=F32)
-            acc = acc + jnp.dot(hidden[1], down_w[1, :, cols], preferred_element_type=F32)
-            y[q, :, :, cols] = acc.astype(BF16).reshape(nsp, cap, tile)
+            cols = pl.ds(pl.multiple_of(j * wide, wide), wide)
+            acc = jnp.dot(hidden[0, filled], down_w[0, :, cols], preferred_element_type=F32)
+            acc = acc + jnp.dot(hidden[1, filled], down_w[1, :, cols], preferred_element_type=F32)
+            y[pl.ds(q, n), :, :, cols] = acc.astype(BF16).reshape(n, nsp, cap, wide)
             return carry
 
-        lax.fori_loop(0, width // tile, columns, 0)
-
-    def experts(q):
-        all_in(x, q, ahead, plane_recv.at[q])
-        ffn(q)
-        over_plane(y, back_at, q, ahead, back_send.at[q], back_recv.at[q])
+        lax.fori_loop(0, width // wide, columns, 0)
+
+    def experts(q, n):
+        for i in range(n):
+            all_in(x, q + i, ahead, plane_recv.at[q + i])
+        ffn(q, n)
+        for i in range(n):
+            over_plane(y, back_at, q + i, ahead, back_send.at[q + i], back_recv.at[q + i])
+
+    def arm(way, r):
+        k = far - r
+        if k == 0 or k == far:
+            return 0 if k == 0 else 2 * far - 1
+        return 2 * k if way == 0 else 2 * k - 1
+
+    landed = (from_left, from_right)
+
+    def reduce(way, r, h):
+        return remote(
+            half(y, arm(way, r), h),
+            half(landed[way], r, h),
+            rs_send.at[way, r, h],
+            rs_recv.at[way, r, h],
+            s,
+            right if way == 0 else left,
+        )
+
+    def moves(way, r, h):
+        return r > 0 or h != way
+
+    def open_arms(copy):
+        for way in (0, 1):
+            copy(way, 0, 1 - way).start()
+
+    def second_halves(copy):
+        if far > 1:
+            for way in (0, 1):
+                copy(way, 1, way).start()
 
     start_hop(gather, 0)
     for k in range(2, far + 1):
@@ -475,31 +508,12 @@
         pltpu.make_async_copy(src.at[0], dst.at[0], own_sem.at[i]).wait()
     for i in range(3):
         to_mate(i).wait_recv()
-    q_loop(0, 1, experts)
+    experts(0, 1)
     for k in range(1, far + 1):
         pass_on(gather, k)
-        q_loop(2 * k - 1, min(2 * k + 1, nz), experts)
-
-    def arm(way, r):
-        k = far - r
-        if k == 0 or k == far:
-            return 0 if k == 0 else 2 * far - 1
-        return 2 * k if way == 0 else 2 * k - 1
-
-    landed = (from_left, from_right)
-
-    def reduce(way, r, h):
-        return remote(
-            half(y, arm(way, r), h),
-            half(landed[way], r, h),
-            rs_send.at[way, r, h],
-            rs_recv.at[way, r, h],
-            s,
-            right if way == 0 else left,
-        )
-
-    def moves(way, r, h):
-        return r > 0 or h != way
+        experts(2 * k - 1, 2 if k < far else 1)
+        if k == far - 1:
+            second_halves(reduce)
 
     def add(q, buf, r, h):
         rows = pl.ds(h * hs, hs)
@@ -537,15 +551,6 @@
             sums[q, :, :, cols] = mixed.astype(BF16).reshape(2, ht, tile)
 
         column_loop(0, early, body)
-
-    def open_arms(copy):
-        for way in (0, 1):
-            copy(way, 0, 1 - way).start()
-
-    def second_halves(copy):
-        if far > 1:
-            for way in (0, 1):
-                copy(way, 1, way).start()
 
     def advance(copy, plus, bufs, r):
         for h in (0, 1):
@@ -558,7 +563,6 @@
                 copy(way, r, hh).start()
 
     open_arms(reduce)
-    second_halves(reduce)
     q_loop(nz - 1, nz, combine)
     open_arms(reduce_sums)
     if far > 1:
@@ -686,7 +690,7 @@
     dma = pltpu.SemaphoreType.DMA
     return pl.pallas_call(
         functools.partial(kernel, nsp, nz, early),
-        out_shape=jax.ShapeDtypeStruct((tokens, width), BF16),
+        out_shape=pltpu.VMEM((tokens, width), BF16),
         in_specs=[vmem] * 5 + [hbm] * 2 + [vmem] * 3 + [hbm] * 3,
         out_specs=vmem,
         scratch_shapes=[
@@ -703,7 +707,7 @@
             pltpu.VMEM((2, hid, width), BF16),
             pltpu.VMEM((2, hid, width), BF16),
             pltpu.VMEM((2, hid, width), BF16),
-            pltpu.VMEM((2, nsp * cap, hid), BF16),
+            pltpu.VMEM((2, 2 * nsp * cap, hid), BF16),
             pltpu.VMEM((nz, 8, lanes), F32),
             pltpu.VMEM((nz, 2, tokens // 2, early), BF16),
             pltpu.VMEM((nz, nsp, cap, width), BF16),

time: 111 us -> 104 us (0.937)
  Pallas kernels: 109 us -> 103 us
    pallas_call x1, Pallas kernels: 109 us -> 103 us  [per_device(): pl.pallas_call(functools.partial(kernel, nsp, nz, early), out_shape=pltpu...]
where the time goes in v4:
time: 104 us
  Pallas kernels  103 us (99%)
    pallas_call x1, Pallas kernels, per_device(): pl.pallas_call(functools.partial(kernel, nsp, nz, early), out_shape=pltpu...  103 us

profile of v4, /device:TPU:2, one launch (start us, length us, event | category | flops | bytes accessed | tf_op | source)
XLA Modules:
  0.0 103.6 jit_solution(8421630043145087994)
XLA Ops:
  0.0 102.9 %block.1 = bf16[64,2048]{1,0:T(8,128)(2,1)S(1)} custom-call(bf16[64,1024]{1,0:T(8,128)(2,1)} %value_ref.1, bf16[64,1024]{1,0:T(8,128)(2,1)} %gating_ref.1, f32[31,64]{1,0:T(8,128)} %bitcast.12, f32[1,1024]{1,0:T(1,128)} %bitcast.14, f32[1,1024]{1,0:T(1,128)} %bitcast.15, bf16[16,2,32,2048]{3,2,1,0:T(8,128)(2,1)} %bitcast.9, bf16[64,2048]{1,0:T(8,128)(2,1)} %stream_ref.1, ...), custom_call_target="tpu_custom_call" | custom-call | tf_op jit(solution)/shard_map/block/pallas_call | solution.py:691
  102.9 0.7 copy.15

commit v5 on v4

--- a/solution.py
+++ b/solution.py
@@ -238,7 +238,7 @@
     low_lanes = lax.broadcasted_iota(jnp.int32, (sub, lanes), 1) < tokens
 
     def conv_tile(i, carry):
-        p = nz - 1 - i
+        p = jnp.where(i == nz - 1, 0, 1 + lax.rem(z + i, nz - 1))
 
         @pl.when(p == 0)
         def _():
@@ -501,9 +501,12 @@
                 copy(way, 1, way).start()
 
     start_hop(gather, 0)
-    for k in range(2, far + 1):
-        pass_on(spread, k)
-        q_loop(2 * k - 1, min(2 * k + 1, nz), select)
+    def spread_and_select(k):
+        if k <= far:
+            pass_on(spread, k)
+            q_loop(2 * k - 1, min(2 * k + 1, nz), select)
+
+    spread_and_select(2)
     for i, (src, dst) in enumerate(pairs):
         pltpu.make_async_copy(src.at[0], dst.at[0], own_sem.at[i]).wait()
     for i in range(3):
@@ -511,6 +514,7 @@
     experts(0, 1)
     for k in range(1, far + 1):
         pass_on(gather, k)
+        spread_and_select(k + 2)
         experts(2 * k - 1, 2 if k < far else 1)
         if k == far - 1:
             second_halves(reduce)
@@ -562,35 +566,44 @@
                 plus(arm(way, r), bufs[way], r - 1, hh)
                 copy(way, r, hh).start()
 
+    def finish_reduce():
+        for h in (0, 1):
+            rows = pl.ds(h * hs, hs)
+            for way in (0, 1):
+                if moves(way, far - 1, h):
+                    reduce(way, far - 1, h).wait_recv()
+
+            def finish(cols):
+                total = y[0, rows, :, cols].astype(F32)
+                for way in (0, 1):
+                    if moves(way, far - 1, h):
+                        total = total + landed[way][far - 1, rows, :, cols].astype(F32)
+                final[0, rows, :, cols] = total.astype(BF16)
+
+            column_loop(early, width, finish)
+
+        over_plane(final, returned, 0, late, ret_send.at[0], ret_recv.at[0])
+
     open_arms(reduce)
+    if far > 1:
+        advance(reduce, add, landed, 1)
     q_loop(nz - 1, nz, combine)
     open_arms(reduce_sums)
     if far > 1:
         q_loop(nz - 3, nz - 1, combine)
         second_halves(reduce_sums)
     for r in range(1, far):
-        advance(reduce, add, landed, r)
         if r + 1 < far:
+            advance(reduce, add, landed, r + 1)
             q_loop(nz - 3 - 2 * r, nz - 1 - 2 * r, combine)
+        else:
+            q_loop(0, 1, combine)
+            finish_reduce()
         advance(reduce_sums, add_sums, sums_landed, r)
-    q_loop(0, 1, combine)
-
-    for h in (0, 1):
-        rows = pl.ds(h * hs, hs)
-        for way in (0, 1):
-            if moves(way, far - 1, h):
-                reduce(way, far - 1, h).wait_recv()
-
-        def finish(cols):
-            total = y[0, rows, :, cols].astype(F32)
-            for way in (0, 1):
-                if moves(way, far - 1, h):
-                    total = total + landed[way][far - 1, rows, :, cols].astype(F32)
-            final[0, rows, :, cols] = total.astype(BF16)
-
-        column_loop(early, width, finish)
-
-    over_plane(final, returned, 0, late, ret_send.at[0], ret_recv.at[0])
+    if far == 1:
+        q_loop(0, 1, combine)
+        finish_reduce()
+
 
     for h in (0, 1):
         rows = pl.ds(h * ht, ht)

time: 104 us -> 100 us (0.962)
  Pallas kernels: 103 us -> 98.8 us
    pallas_call x1, Pallas kernels: 103 us -> 98.8 us  [per_device(): pl.pallas_call(functools.partial(kernel, nsp, nz, early), out_shape=pltpu...]
where the time goes in v5:
time: 100 us; the launch traced here: 99.5 us
  Pallas kernels  98.8 us (99%)
    pallas_call x1, Pallas kernels, per_device(): pl.pallas_call(functools.partial(kernel, nsp, nz, early), out_shape=pltpu...  98.8 us

profile of v5, /device:TPU:2, one launch (start us, length us, event | category | flops | bytes accessed | tf_op | source)
XLA Modules:
  0.0 99.5 jit_solution(558621018610683087)
XLA Ops:
  0.0 98.8 %block.1 = bf16[64,2048]{1,0:T(8,128)(2,1)S(1)} custom-call(bf16[64,1024]{1,0:T(8,128)(2,1)} %value_ref.1, bf16[64,1024]{1,0:T(8,128)(2,1)} %gating_ref.1, f32[31,64]{1,0:T(8,128)} %bitcast.12, f32[1,1024]{1,0:T(1,128)} %bitcast.14, f32[1,1024]{1,0:T(1,128)} %bitcast.15, bf16[16,2,32,2048]{3,2,1,0:T(8,128)(2,1)} %bitcast.9, bf16[64,2048]{1,0:T(8,128)(2,1)} %stream_ref.1, ...), custom_call_target="tpu_custom_call" | custom-call | tf_op jit(solution)/shard_map/block/pallas_call | solution.py:704
  98.8 0.7 copy.15
